TPU v7x, 32 devices: a whole 2x2x4 slice. The times are simulated.
32 devices in a mesh: sp: 8 (over z, x), tp: 4 (over y, core).
Axes of the slice: x: 2, y: 2, z: 4, core: 2. Of those that a mesh axis runs over, the one named last changes fastest.
Arguments:
- inputs: bfloat16 [4096, 2048], P(('sp', 'tp')), may hold values from -6 to 6
- norm_gain: float32 [2048], replicated, may hold values from 0.1 to 1.9
- w_query: bfloat16 [2048, 1024], P(None, 'tp'), may hold values from -1 to 1
- w_key: bfloat16 [2048, 1024], P(None, 'tp'), may hold values from -1 to 1
- w_value: bfloat16 [2048, 1024], P(None, 'tp'), may hold values from -0.125 to 0.125
- query_gain: float32 [2, 64], replicated, may hold values from 1 to 5.5
- key_gain: float32 [2, 64], replicated, may hold values from 1 to 5.5
- lambdas: float32 [8], P('tp'), may hold values from 0.3 to 0.8
- sub_gain: float32 [128], replicated, may hold values from 0.1 to 1.9
- w_gate_b: bfloat16 [2048, 1024], P(None, 'tp'), may hold values from -0.125 to 0.125
- w_gate_c: bfloat16 [2048, 1024], P(None, 'tp'), may hold values from -0.125 to 0.125
- w_conv_in: bfloat16 [2048, 1024], P(None, 'tp'), may hold values from -0.125 to 0.125
- conv_taps: float32 [3, 1024], P(None, 'tp'), may hold values from -3 to 3
- conv_gain: float32 [1024], P('tp'), may hold values from 0.1 to 1.9
- w_out_att: bfloat16 [1024, 2048], P('tp'), may hold values from -0.125 to 0.125
- w_out_conv: bfloat16 [1024, 2048], P('tp'), may hold values from -0.125 to 0.125
Outputs:
- mixed: float32 [4096, 2048], P(('sp', 'tp'))
- log_sums: float32 [8, 2, 4096], P('tp', None, 'sp')
All inputs are finite; a program needn't handle non-finite values.
Results may differ from a plain program's by a relative error of at most 0.034.
Values may be sent and summed in bfloat16 or wider, within the bound.
A program may use at most 192 MiB of HBM per device.

v0:
```python
import functools

import jax
import jax.numpy as jnp
from jax import lax
from jax.experimental import pallas as pl
from jax.experimental.pallas import tpu as pltpu
from jax.sharding import PartitionSpec as P

GROUP = 64
eps = 1e-06
MESH = pl.DeviceIdType.MESH
VMEM_LIMIT = 60 * 1024 * 1024


def rms_scale(values):
    return values * lax.rsqrt(jnp.mean(values * values, axis=-1, keepdims=True) + eps)


def flip(index, bit):
    return index + bit - 2 * bit * lax.rem(index // bit, 2)


def remote(src, dst, send, recv, axis, target):
    return pltpu.make_async_remote_copy(
        src_ref=src,
        dst_ref=dst,
        send_sem=send,
        recv_sem=recv,
        device_id={axis: target},
        device_id_type=MESH,
    )


def greet(axis, targets):
    barrier = pltpu.get_barrier_semaphore()
    for target in targets:
        pl.semaphore_signal(barrier, inc=1, device_id={axis: target}, device_id_type=MESH)
    pl.semaphore_wait(barrier, len(targets))


CHUNKS = 4
HALVES = 2


def group_scale(values, size):
    lanes = values.shape[1]
    row = lax.broadcasted_iota(jnp.int32, (lanes, lanes), 0) // size
    col = lax.broadcasted_iota(jnp.int32, (lanes, lanes), 1) // size
    ones = jnp.where(row == col, 1.0, 0.0).astype(jnp.bfloat16)
    squares = values * values
    high = squares.astype(jnp.bfloat16)
    low = (squares - high.astype(jnp.float32)).astype(jnp.bfloat16)
    sums = jnp.dot(high, ones, preferred_element_type=jnp.float32) + jnp.dot(
        low, ones, preferred_element_type=jnp.float32
    )
    return lax.rsqrt(sums * (1.0 / size) + eps)


def gather_project(comp, x_ref, gain_ref, qk_ref, *rest):
    weights = rest[:6]
    q_ref, kv_ref, conv_ref, held, wbuf = rest[6:11]
    wsem, far_send, far_recv, near_sem, fwd_send, fwd_recv = rest[11:]
    me = lax.axis_index("tp")
    near, far = flip(me, 1), flip(me, 2)
    diag = flip(near, 2)
    rows = x_ref.shape[0]
    wcols = wbuf.shape[2]
    loads = [pltpu.make_async_copy(w, wbuf.at[i], wsem.at[i]) for i, w in enumerate(weights)]
    for load in loads:
        load.start()
    x = x_ref[...].astype(jnp.float32)
    held[me] = (rms_scale(x) * gain_ref[...]).astype(jnp.bfloat16)
    greet("tp", (near, far))
    part = rows // CHUNKS

    def far_copy(c):
        spot = held.at[me, pl.ds(c * part, part)]
        return remote(spot, spot, far_send.at[c], far_recv.at[c], "tp", far)

    def forward(c):
        spot = held.at[far, pl.ds(c * part, part)]
        return remote(spot, spot, fwd_send.at[c], fwd_recv.at[c], "tp", near)

    far_copies = [far_copy(c) for c in range(CHUNKS)]
    forwards = [forward(c) for c in range(CHUNKS)]
    near_copy = remote(held.at[me], held.at[me], near_sem.at[0], near_sem.at[1], "tp", near)
    for copy in far_copies:
        copy.start()
    near_copy.start()

    def project(slot):
        block = held[slot]
        at = pl.ds(pl.multiple_of(slot * rows, rows), rows)
        for i in range(6):
            res = jnp.dot(block, wbuf[i], preferred_element_type=jnp.float32).astype(jnp.bfloat16)
            if i < 2:
                wide = res.astype(jnp.float32)
                wide = wide * group_scale(wide, comp) * qk_ref[i : i + 1]
                res = wide.astype(jnp.bfloat16)
            if i == 0:
                q_ref[at, :] = res
            elif i < 3:
                kv_ref[at, (i - 1) * wcols : i * wcols] = res
            else:
                conv_ref[at, (i - 3) * wcols : (i - 2) * wcols] = res

    for load in loads:
        load.wait()
    project(me)
    near_copy.wait_recv()
    project(near)
    for c in range(CHUNKS):
        far_copies[c].wait_recv()
        forwards[c].start()
    project(far)
    for copy in forwards:
        copy.wait_recv()
    project(diag)
    near_copy.wait_send()
    for copy in far_copies + forwards:
        copy.wait_send()


def attend(
    heads, q_ref, kv_ref, lam_ref, sub_ref, proj_ref, taps_ref, cgain_ref, out_ref, log_ref,
    conv_ref, buf, qpad, top, total, acc, tail, padded, up_send, side_send, recv, tail_sem,
):
    n = buf.shape[0]
    me = lax.axis_index("sp")
    z, x = me // 2, lax.rem(me, 2)
    levels = n // 2
    partner = z * 2 + 1 - x
    rows = q_ref.shape[0]
    both = q_ref.shape[1] // heads
    comp = both // 2
    vsize = sub_ref.shape[0]
    barrier = pltpu.get_barrier_semaphore()
    has_up, has_down = z < levels - 1, z > 0
    pl.semaphore_signal(barrier, inc=1, device_id={"sp": partner}, device_id_type=MESH)

    @pl.when(has_up)
    def _():
        pl.semaphore_signal(barrier, inc=1, device_id={"sp": me + 2}, device_id_type=MESH)

    @pl.when(has_down)
    def _():
        pl.semaphore_signal(barrier, inc=1, device_id={"sp": me - 2}, device_id_type=MESH)

    ups, downs = has_up.astype(jnp.int32), has_down.astype(jnp.int32)

    @pl.when((x == 1) & has_up)
    def _():
        pl.semaphore_signal(barrier, inc=1, device_id={"sp": me + 1}, device_id_type=MESH)

    @pl.when((x == 0) & has_down)
    def _():
        pl.semaphore_signal(barrier, inc=1, device_id={"sp": me - 1}, device_id_type=MESH)

    pl.semaphore_wait(barrier, 1 + ups + downs + x * ups + (1 - x) * downs)
    edge = tail.shape[0]
    channels = conv_ref.shape[1]
    tail_copy = remote(
        proj_ref.at[pl.ds(rows - edge, edge), pl.ds(channels, 2 * channels)], tail,
        tail_sem.at[0], tail_sem.at[1], "sp", jnp.minimum(me + 1, n - 1),
    )
    size = rows // HALVES

    def up_copy(src, block, half):
        at = pl.ds(half * size, size)
        return remote(
            src.at[at], buf.at[block, at], up_send.at[block // 2, half], recv.at[block, half],
            "sp", jnp.minimum(me + 2, n - 2 + x),
        )

    def side_copy(src, block, half):
        at = pl.ds(half * size, size)
        return remote(
            src.at[at], buf.at[block, at], side_send.at[block // 2, half], recv.at[block, half],
            "sp", partner,
        )

    @pl.when(has_up)
    def _():
        for half in range(HALVES):
            up_copy(kv_ref, me, half).start()

    @pl.when(x == 0)
    def _():
        for half in range(HALVES):
            side_copy(kv_ref, me, half).start()

    @pl.when(me < n - 1)
    def _():
        tail_copy.start()

    lane = lax.broadcasted_iota(jnp.int32, (rows, both), 1)
    for h in range(heads):
        q = q_ref[:, h * both : (h + 1) * both]
        zero = jnp.zeros_like(q)
        qpad[h, :rows] = jnp.where(lane < comp, q, zero)
        qpad[h, rows:] = jnp.where(lane < comp, zero, q)
    top[...] = jnp.full_like(top, -1e30)
    total[...] = jnp.zeros_like(total)
    acc[...] = jnp.zeros_like(acc)
    tile = min(256, rows)

    def absorb(piece, masked):
        for h in range(heads):
            for start in range(0, 2 * rows, tile):
                first = start % rows
                keys = first + tile if masked else rows
                k = piece[:keys, h * both : (h + 1) * both]
                v = piece[:keys, heads * both + h * vsize : heads * both + (h + 1) * vsize]
                at = slice(start, start + tile)
                s = lax.dot_general(
                    k, qpad[h, at], (((1,), (1,)), ((), ())), preferred_element_type=jnp.float32
                )
                if masked:
                    kpos = lax.broadcasted_iota(jnp.int32, s.shape, 0)
                    qpos = first + lax.broadcasted_iota(jnp.int32, s.shape, 1)
                    s = jnp.where(kpos <= qpos, s, -1e30)
                old = top[h : h + 1, at]
                new = jnp.maximum(old, jnp.max(s, axis=0, keepdims=True))
                p = jnp.exp(s - new)
                factor = jnp.exp(old - new)
                top[h : h + 1, at] = new
                total[h : h + 1, at] = total[h : h + 1, at] * factor + jnp.sum(
                    p, axis=0, keepdims=True
                )
                acc[h, :, at] = acc[h, :, at] * factor + lax.dot_general(
                    v, p.astype(jnp.bfloat16), (((0,), (0,)), ((), ())),
                    preferred_element_type=jnp.float32,
                )

    absorb(kv_ref, True)

    def product(ref, at):
        gate = ref[:, at : at + channels].astype(jnp.float32)
        other = ref[:, at + channels : at + 2 * channels].astype(jnp.float32)
        return (gate * other).astype(jnp.bfloat16).astype(jnp.float32)

    padded[edge:] = product(proj_ref, channels)

    @pl.when(me > 0)
    def _():
        tail_copy.wait_recv()
        padded[:edge] = product(tail, 0)

    @pl.when(me == 0)
    def _():
        padded[:edge] = jnp.zeros((edge, channels), jnp.float32)

    count = taps_ref.shape[0]
    conv = jnp.zeros((rows, channels), jnp.float32)
    for tap in range(count):
        first = edge - count + 1 + tap
        conv = conv + taps_ref[tap : tap + 1] * padded[first : first + rows]
    gated = proj_ref[:, :channels].astype(jnp.float32) * conv
    conv_ref[...] = (gated * group_scale(gated, GROUP) * cgain_ref[...]).astype(jnp.bfloat16)

    @pl.loop(0, 2 * (z + 1))
    def _(j):
        step, other = j // 2 + 1, lax.rem(j, 2)
        level = z - step + other
        block = jnp.maximum(level, 0) * 2 + x + other * (1 - 2 * x)
        valid = jnp.where(other == 0, step <= z, (x == 1) | (step >= 2))

        @pl.when(valid)
        def _():
            for half in range(HALVES):
                side_copy(buf.at[block], block, half).wait_recv()

                @pl.when(other == 0)
                def _():
                    @pl.when(has_up)
                    def _():
                        up_copy(buf.at[block], block, half).start()

                    side_copy(buf.at[block], block, half).start()

            absorb(buf.at[block], False)

    for h in range(heads):
        mapped = acc[h] / total[h : h + 1]
        attn = mapped[:, :rows] - lam_ref[h] * mapped[:, rows:]
        scale = lax.rsqrt(jnp.mean(attn * attn, axis=0, keepdims=True) + eps)
        result = attn * scale * sub_ref[...]
        out_ref[:, h * vsize : (h + 1) * vsize] = result.T.astype(jnp.bfloat16)
        logs = top[h : h + 1] + jnp.log(total[h : h + 1])
        log_ref[h, 0:1, :] = logs[:, :rows]
        log_ref[h, 1:2, :] = logs[:, rows:]

    @pl.loop(0, z + 1)
    def _(level):
        block = level * 2 + x

        @pl.when(has_up)
        def _():
            for half in range(HALVES):
                up_copy(kv_ref, block, half).wait_send()

        @pl.when((x == 0) | (level < z))
        def _():
            for half in range(HALVES):
                side_copy(kv_ref, block, half).wait_send()

    @pl.when(me < n - 1)
    def _():
        tail_copy.wait_send()


def project_scatter(
    heads_ref, conv_ref, wa_ref, wc_ref, out_ref, cross, fin, far, cross_in, fin_in, far_in,
    cross_send, cross_recv, fin_send, fin_recv, far_send, far_recv,
):
    me = lax.axis_index("tp")
    near, other = flip(me, 1), flip(me, 2)
    diag = flip(near, 2)
    rows = out_ref.shape[0]
    width = out_ref.shape[1] // CHUNKS
    greet("tp", (near, other))

    def partial(target, c):
        at = pl.ds(pl.multiple_of(target * rows, rows), rows)
        cols = slice(c * width, (c + 1) * width)
        return jnp.dot(
            heads_ref[at, :], wa_ref[:, cols], preferred_element_type=jnp.float32
        ) + jnp.dot(conv_ref[at, :], wc_ref[:, cols], preferred_element_type=jnp.float32)

    crosses = [
        remote(cross.at[c], cross_in.at[c], cross_send.at[c], cross_recv.at[c], "tp", near)
        for c in range(CHUNKS)
    ]
    fins = [
        remote(fin.at[c], fin_in.at[c], fin_send.at[c], fin_recv.at[c], "tp", near)
        for c in range(CHUNKS)
    ]
    fars = [
        remote(far.at[c], far_in.at[c], far_send.at[c], far_recv.at[c], "tp", other)
        for c in range(CHUNKS)
    ]
    for c in range(CHUNKS):
        cross[c] = partial(diag, c).astype(jnp.bfloat16)
        crosses[c].start()
    for c in range(CHUNKS):
        mine = partial(other, c)
        crosses[c].wait_recv()
        far[c] = (mine + cross_in[c].astype(jnp.float32)).astype(jnp.bfloat16)
        fars[c].start()
    for c in range(CHUNKS):
        fin[c] = partial(near, c).astype(jnp.bfloat16)
        fins[c].start()
    for c in range(CHUNKS):
        cols = slice(c * width, (c + 1) * width)
        out_ref[:, cols] = partial(me, c)
    for c in range(CHUNKS):
        cols = slice(c * width, (c + 1) * width)
        fins[c].wait_recv()
        fars[c].wait_recv()
        out_ref[:, cols] += fin_in[c].astype(jnp.float32) + far_in[c].astype(jnp.float32)
    for copy in crosses + fins + fars:
        copy.wait_send()


def vmem():
    return pl.BlockSpec(memory_space=pltpu.VMEM)


def on_device(
    inputs, norm_gain, w_query, w_key, w_value, query_gain, key_gain, lambdas, sub_gain,
    w_gate_b, w_gate_c, w_conv_in, conv_taps, conv_gain, w_out_att, w_out_conv,
):
    heads = lambdas.shape[0]
    comp = query_gain.shape[1]
    vsize = sub_gain.shape[0]
    channels = conv_gain.shape[0]
    own, width = inputs.shape
    tp = lax.axis_size("tp")
    sp = lax.axis_size("sp")
    rows = own * tp
    dma = pltpu.SemaphoreType.DMA

    def params(cid):
        return pltpu.CompilerParams(
            collective_id=cid, has_side_effects=True, vmem_limit_bytes=VMEM_LIMIT
        )

    qcols = heads * 2 * comp
    weights = (w_query, w_key, w_value, w_gate_b, w_gate_c, w_conv_in)
    qk_gain = jnp.stack(
        [
            jnp.tile(query_gain.reshape(-1) * comp ** (-0.5), heads),
            jnp.tile(key_gain.reshape(-1), heads),
        ]
    )
    qn, kv, conv_proj = pl.pallas_call(
        functools.partial(gather_project, comp),
        out_shape=(
            jax.ShapeDtypeStruct((rows, qcols), jnp.bfloat16),
            jax.ShapeDtypeStruct((rows, 2 * qcols), jnp.bfloat16),
            jax.ShapeDtypeStruct((rows, 3 * channels), jnp.bfloat16),
        ),
        in_specs=[vmem()] * 3 + [pl.BlockSpec(memory_space=pl.ANY)] * 6,
        out_specs=(vmem(), vmem(), vmem()),
        scratch_shapes=[
            pltpu.VMEM((tp, own, width), jnp.bfloat16),
            pltpu.VMEM((6, width, qcols), jnp.bfloat16),
            dma((6,)), dma((CHUNKS,)), dma((CHUNKS,)), dma((2,)), dma((CHUNKS,)), dma((CHUNKS,)),
        ],
        compiler_params=params(0),
        name="gather_project",
    )(inputs, norm_gain[None], qk_gain, *weights)

    heads_out, log_sums, conv_out = pl.pallas_call(
        functools.partial(attend, heads),
        out_shape=(
            jax.ShapeDtypeStruct((rows, heads * vsize), jnp.bfloat16),
            jax.ShapeDtypeStruct((heads, 2, rows), jnp.float32),
            jax.ShapeDtypeStruct((rows, channels), jnp.bfloat16),
        ),
        in_specs=[vmem(), vmem(), pl.BlockSpec(memory_space=pltpu.SMEM)] + [vmem()] * 4,
        out_specs=(vmem(), vmem(), vmem()),
        scratch_shapes=[
            pltpu.VMEM((sp, rows, kv.shape[1]), jnp.bfloat16),
            pltpu.VMEM((heads, 2 * rows, 2 * comp), jnp.bfloat16),
            pltpu.VMEM((heads, 2 * rows), jnp.float32),
            pltpu.VMEM((heads, 2 * rows), jnp.float32),
            pltpu.VMEM((heads, vsize, 2 * rows), jnp.float32),
            pltpu.VMEM((16, 2 * channels), jnp.bfloat16),
            pltpu.VMEM((16 + rows, channels), jnp.float32),
            dma((sp // 2, HALVES)), dma((sp // 2, HALVES)), dma((sp, HALVES)), dma((2,)),
        ],
        compiler_params=params(1),
        cost_estimate=pl.CostEstimate(flops=20_000_000_000, bytes_accessed=0, transcendentals=0),
        name="attend",
    )(qn, kv, lambdas, sub_gain[:, None], conv_proj, conv_taps, conv_gain[None])

    piece = pltpu.VMEM((CHUNKS, own, width // CHUNKS), jnp.bfloat16)
    mixed = pl.pallas_call(
        project_scatter,
        out_shape=jax.ShapeDtypeStruct((own, width), jnp.float32),
        in_specs=[vmem()] * 4,
        out_specs=vmem(),
        scratch_shapes=[piece] * 6 + [dma((CHUNKS,))] * 6,
        compiler_params=params(2),
        name="project_scatter",
    )(heads_out, conv_out, w_out_att, w_out_conv)
    return (mixed, log_sums)


def solution(mesh):
    in_specs = (
        P(("sp", "tp"), None),
        P(),
        P(None, "tp"),
        P(None, "tp"),
        P(None, "tp"),
        P(),
        P(),
        P("tp"),
        P(),
        P(None, "tp"),
        P(None, "tp"),
        P(None, "tp"),
        P(None, "tp"),
        P("tp"),
        P("tp", None),
        P("tp", None),
    )
    out_specs = (P(("sp", "tp"), None), P("tp", None, "sp"))
    return jax.shard_map(
        on_device, mesh=mesh, in_specs=in_specs, out_specs=out_specs, check_vma=False
    )
```

profile of v0, /device:TPU:24, one launch (start us, length us, event | category | flops | bytes accessed | tf_op | source)
XLA Modules:
  0.0 101.0 jit_solution(5281465469342993662)
XLA Ops:
  0.6 0.0 copy-start.3
  0.6 0.7 copy-done.3
  1.3 0.1 tile.14
  1.4 0.0 copy-start.1
  1.4 0.7 copy-done.1
  2.1 0.1 mul.15
  2.2 0.0 copy-start.2
  2.2 0.6 pad_maximum_fusion.qk_ref
  2.8 0.1 copy-done.2
  2.8 0.7 copy.18.sub_ref
  3.6 19.9 %gather_project.1 = (bf16[512,256]{1,0:T(8,128)(2,1)}, bf16[512,512]{1,0:T(8,128)(2,1)}, bf16[512,768]{1,0:T(8,128)(2,1)}) custom-call(bf16[128,2048]{1,0:T(8,128)(2,1)} %x_ref.1, f32[1,2048]{1,0:T(1,128)} %bitcast.5, f32[2,256]{1,0:T(2,128)} %pad_maximum_fusion.qk_ref, bf16[2048,256]{1,0:T(8,128)(2,1)} %rest_0_.1, bf16[2048,256]{1,0:T(8,128)(2,1)} %rest_1_.1, ...), custom_call_target="tpu_custom_call" | custom-call | tf_op jit(solution)/shard_map/gather_project/pallas_call | solution.py:397
  23.5 55.9 %attend.1 = (bf16[512,256]{1,0:T(8,128)(2,1)}, f32[2,2,512]{2,1,0:T(2,128)}, bf16[512,256]{1,0:T(8,128)(2,1)}) custom-call(bf16[512,256]{1,0:T(8,128)(2,1)} %get-tuple-element.8.q_ref, bf16[512,512]{1,0:T(8,128)(2,1)} %get-tuple-element.9.kv_ref, f32[2]{0:T(128)} %lam_ref.1, f32[128,1]{1,0:T(8,128)} %copy.18.sub_ref, ...), custom_call_target="tpu_custom_call" | custom-call | flops 20000000000 | tf_op jit(solution)/shard_map/attend/pallas_call | solution.py:415
  79.4 18.7 %project_scatter.1 = f32[128,2048]{1,0:T(8,128)} custom-call(bf16[512,256]{1,0:T(8,128)(2,1)} %get-tuple-element.11.heads_ref, bf16[512,256]{1,0:T(8,128)(2,1)} %get-tuple-element.12.conv_ref, bf16[256,2048]{1,0:T(8,128)(2,1)} %wa_ref.1, bf16[256,2048]{1,0:T(8,128)(2,1)} %wc_ref.1), custom_call_target="tpu_custom_call" | custom-call | tf_op jit(solution)/shard_map/project_scatter/pallas_call | solution.py:440
  98.1 0.0 copy-start
  98.1 2.3 %copy.21 = f32[128,2048]{1,0:T(8,128)} copy(f32[128,2048]{1,0:T(8,128)} %project_scatter.1) | data formatting | bytes 2097152
  100.4 0.0 copy-done
  100.4 0.6 copy.22
  (3 shorter events, 0.0 us)
Async XLA Ops:
  0.6 0.7 copy-start.3
  1.4 0.7 copy-start.1
  2.2 0.7 copy-start.2
  98.1 2.3 %copy-start = (f32[2,2,512]{2,1,0:T(2,128)S(1)}, f32[2,2,512]{2,1,0:T(2,128)}, u32[]{:S(2)}) copy-start(f32[2,2,512]{2,1,0:T(2,128)} %get-tuple-element.17) | copy-start | bytes 24580
where the time goes:
time: 101 us
  Pallas kernels  94.5 us (94%)
  local copies, waits for them, and re-layouts  5.24 us (5%)
    pallas_call x1, Pallas kernels, on_device(): pl.pallas_call(functools.partial(attend, heads), out_shape=(jax.ShapeDtyp...  55.9 us
    pallas_call x1, Pallas kernels, on_device(): pl.pallas_call(functools.partial(gather_project, comp), out_shape=(jax.Sh...  19.9 us
    pallas_call x1, Pallas kernels, on_device(): pl.pallas_call(project_scatter, out_shape=jax.ShapeDtypeStruct((own, widt...  18.7 us
    unnamed x10, local copies, waits for them, and re-layouts  4.33 us

commit v1 on v0

v1 whole, which is shorter than its diff:
```python
import functools

import jax
import jax.numpy as jnp
from jax import lax
from jax.experimental import pallas as pl
from jax.experimental.pallas import tpu as pltpu
from jax.sharding import PartitionSpec as P

GROUP = 64
eps = 1e-06
MESH = pl.DeviceIdType.MESH
VMEM_LIMIT = 62 * 1024 * 1024
CHUNKS = 4
EDGE = 16
TILE = 256


def rms_scale(values):
    return values * lax.rsqrt(jnp.mean(values * values, axis=-1, keepdims=True) + eps)


def flip(index, bit):
    return index + bit - 2 * bit * lax.rem(index // bit, 2)


def remote(src, dst, send, recv, where):
    return pltpu.make_async_remote_copy(
        src_ref=src, dst_ref=dst, send_sem=send, recv_sem=recv, device_id=where,
        device_id_type=MESH,
    )


def group_scale(values, size):
    lanes = values.shape[1]
    row = lax.broadcasted_iota(jnp.int32, (lanes, lanes), 0) // size
    col = lax.broadcasted_iota(jnp.int32, (lanes, lanes), 1) // size
    ones = jnp.where(row == col, 1.0, 0.0).astype(jnp.bfloat16)
    squares = values * values
    high = squares.astype(jnp.bfloat16)
    low = (squares - high.astype(jnp.float32)).astype(jnp.bfloat16)
    sums = jnp.dot(high, ones, preferred_element_type=jnp.float32) + jnp.dot(
        low, ones, preferred_element_type=jnp.float32
    )
    return lax.rsqrt(sums * (1.0 / size) + eps)


def layer(
    sp, tp, comp, heads,
    x_ref, gain_ref, qg_ref, kg_ref, lam_ref, sub_ref, taps_ref, cgain_ref,
    wk, wv, wq, wc, wi, wb, wa, wo,
    out_ref, log_ref,
    held, wbuf, wfull, wobuf, gains, kvb, qb, give_kv, give_q, qpad, top, total, acc, cbuf, tail,
    padded, cvout, cross, fin, far, cross_in, fin_in, far_in, obuf, hin, lout, lin,
    wsem, near_sem, far_send, far_recv, fwd_send, fwd_recv, up_send, kv_recv, gk_send, gq_send,
    q_recv, tail_sem, w_send, w_recv, cross_send, cross_recv, fin_send, fin_recv, fs_send, fs_recv,
    o_send, o_recv, log_sem,
):
    s = lax.axis_index("sp")
    t = lax.axis_index("tp")
    level, side = s // 2, lax.rem(s, 2)
    levels = sp // 2
    mate = level * 2 + 1 - side
    near, away = flip(t, 1), flip(t, 2)
    diag = flip(near, 2)
    first, second = t // 2, 1 - t // 2
    own = x_ref.shape[0]
    rows = own * tp
    half = rows // 2
    head_cols = heads * 2 * comp // 2
    per = heads // 2
    vsize = sub_ref.shape[1]
    both = 2 * comp
    channels = cgain_ref.shape[1]
    has_up, has_down = level < levels - 1, level > 0
    ups, downs = has_up.astype(jnp.int32), has_down.astype(jnp.int32)
    up_id = {"sp": jnp.minimum(s + 2, sp - 2 + side)}
    mate_id = {"sp": mate}

    loads = [
        pltpu.make_async_copy(w, wbuf.at[i], wsem.at[i])
        for i, w in enumerate((wk, wv, wq, wc, wi, wb))
    ]
    for load in loads:
        load.start()
    wa_rows = wa.shape[0]
    half_rows = wa_rows // 2

    def shard(index):
        return pl.ds(pl.multiple_of(index * wa_rows, wa_rows), wa_rows)

    def part_of(index, which):
        return pl.ds(
            pl.multiple_of(index * wa_rows + which * half_rows, half_rows), half_rows
        )

    load_wa = pltpu.make_async_copy(wa, wfull.at[shard(t)], wsem.at[6])
    load_wo = pltpu.make_async_copy(wo, wobuf, wsem.at[7])
    load_wa.start()
    load_wo.start()

    def block_at(index):
        return pl.ds(pl.multiple_of(index * own, own), own)

    x = x_ref[...].astype(jnp.float32)
    held[block_at(t), :] = (rms_scale(x) * gain_ref[...]).astype(jnp.bfloat16)
    for row, ref in ((0, kg_ref), (1, qg_ref)):
        for h in range(heads):
            for m in range(2):
                at = (h * 2 + m) * comp
                gains[row : row + 1, at : at + comp] = ref[m : m + 1, :]

    barrier = pltpu.get_barrier_semaphore()

    def hello(where):
        pl.semaphore_signal(barrier, inc=1, device_id=where, device_id_type=MESH)

    for peer in (near, away, diag):
        hello({"tp": peer})
    for peer in (t, near, away, diag):
        hello({"sp": mate, "tp": peer})

    @pl.when(has_up)
    def _():
        hello({"sp": s + 2})

    @pl.when(has_down)
    def _():
        hello({"sp": s - 2})

    @pl.when((side == 1) & has_up)
    def _():
        hello({"sp": s + 1})

    @pl.when((side == 0) & has_down)
    def _():
        hello({"sp": s - 1})

    pl.semaphore_wait(barrier, 7 + ups + downs + side * ups + (1 - side) * downs)

    part = own // CHUNKS

    def chunk_at(index, c):
        return pl.ds(pl.multiple_of(index * own + c * part, part), part)

    def far_copy(c):
        spot = held.at[chunk_at(t, c)]
        return remote(spot, spot, far_send.at[c], far_recv.at[c], {"tp": away})

    def forward(c):
        spot = held.at[chunk_at(away, c)]
        return remote(spot, spot, fwd_send.at[c], fwd_recv.at[c], {"tp": near})

    far_copies = [far_copy(c) for c in range(CHUNKS)]
    forwards = [forward(c) for c in range(CHUNKS)]
    mine = held.at[block_at(t)]
    near_copy = remote(mine, mine, near_sem.at[0], near_sem.at[1], {"tp": near})
    near_copy.start()
    for copy in far_copies:
        copy.start()

    w_near = remote(wa, wfull.at[shard(t)], w_send.at[0], w_recv.at[0], {"tp": near})
    w_far = remote(
        wa.at[pl.ds(pl.multiple_of(side * half_rows, half_rows), half_rows)],
        wfull.at[part_of(t, side)], w_send.at[1], w_recv.at[1], {"tp": away},
    )

    def w_pass(which, slot):
        spot = wfull.at[part_of(away, which)]
        return remote(spot, spot, w_send.at[slot], w_recv.at[slot], {"tp": near})

    w_side_spot = wfull.at[part_of(away, side)]
    w_side = remote(w_side_spot, w_side_spot, w_send.at[2], w_recv.at[2], mate_id)

    def slot_of(lev, pair):
        return lev * 2 + pair

    def group_of(lev, pair, which):
        return (lev * 2 + pair) * 2 + which

    def side_rows(which):
        return pl.ds(pl.multiple_of(which * half, half), half)

    def up_copy(lev, pair, which):
        spot = kvb.at[slot_of(lev, pair), side_rows(which)]
        g = group_of(lev, pair, which)
        return remote(spot, spot, up_send.at[g], kv_recv.at[g], up_id)

    def give_copy(pair):
        return remote(
            give_kv.at[pair], kvb.at[slot_of(level, pair), side_rows(side)],
            gk_send.at[pair], kv_recv.at[group_of(level, pair, side)], mate_id,
        )

    def q_rows(which, pair):
        return pl.ds(pl.multiple_of(which * rows + pair * half, half), half)

    def giveq_copy(pair):
        return remote(
            give_q.at[pair], qb.at[q_rows(side, pair)], gq_send.at[pair], q_recv.at[pair], mate_id
        )

    def split(values):
        low, high = values[:, :head_cols], values[:, head_cols:]
        return jnp.where(side == 0, low, high), jnp.where(side == 0, high, low)

    def pair_rows(pair):
        return pl.ds(pl.multiple_of(pair * half, half), half)

    def scaled(block, i, gain_row, factor):
        res = jnp.dot(block, wbuf[i], preferred_element_type=jnp.float32).astype(jnp.bfloat16)
        wide = res.astype(jnp.float32)
        return (wide * group_scale(wide, comp) * (gains[gain_row : gain_row + 1] * factor)).astype(
            jnp.bfloat16
        )

    def project_kv(pair):
        block = held[pair_rows(pair)]
        slot = slot_of(level, pair)
        for i in range(2):
            if i == 0:
                res = scaled(block, 0, 0, 1.0)
            else:
                res = jnp.dot(block, wbuf[1], preferred_element_type=jnp.float32).astype(
                    jnp.bfloat16
                )
            keep, give = split(res)
            cols = slice(i * head_cols, (i + 1) * head_cols)
            kvb[slot, side_rows(side), cols] = keep
            give_kv[pair, :, cols] = give

        give_copy(pair).start()

        @pl.when(has_up)
        def _():
            up_copy(level, pair, side).start()

    def project_q(pair):
        block = held[pair_rows(pair)]
        keep, give = split(scaled(block, 2, 1, comp ** (-0.5)))
        qb[q_rows(side, pair)] = keep
        give_q[pair] = give
        giveq_copy(pair).start()

    def project_conv(pair):
        block = held[pair_rows(pair)]
        for i in range(3):
            cbuf[pair_rows(pair), i * channels : (i + 1) * channels] = jnp.dot(
                block, wbuf[3 + i], preferred_element_type=jnp.float32
            ).astype(jnp.bfloat16)

    def await_group(lev, pair, which):
        up_copy(lev, pair, which).wait_recv()

        @pl.when(has_up)
        def _():
            up_copy(lev, pair, which).start()

    def await_pair(lev, pair):
        await_group(lev, pair, side)
        await_group(lev, pair, 1 - side)

    loads[0].wait()
    loads[1].wait()
    near_copy.wait_recv()
    project_kv(first)
    w_near.start()
    w_far.start()
    loads[2].wait()
    project_q(first)
    for load in loads[3:]:
        load.wait()
    project_conv(first)
    await_group(level, first, 1 - side)

    @pl.when(has_down)
    def _():
        await_pair(level - 1, first)

    for c in range(CHUNKS):
        far_copies[c].wait_recv()
        forwards[c].start()
    for copy in forwards:
        copy.wait_recv()
    project_kv(second)
    project_q(second)
    project_conv(second)

    tail_copy = remote(
        cbuf.at[pl.ds(rows - EDGE, EDGE), pl.ds(0, 2 * channels)], tail,
        tail_sem.at[0], tail_sem.at[1], {"sp": jnp.minimum(s + 1, sp - 1)},
    )

    @pl.when(s < sp - 1)
    def _():
        tail_copy.start()

    await_group(level, second, 1 - side)
    giveq_copy(0).wait_recv()
    giveq_copy(1).wait_recv()

    queries = 2 * rows
    lane = lax.broadcasted_iota(jnp.int32, (queries, both), 1)
    for h in range(per):
        q = qb[:, h * both : (h + 1) * both]
        zero = jnp.zeros_like(q)
        qpad[h, :queries] = jnp.where(lane < comp, q, zero)
        qpad[h, queries:] = jnp.where(lane < comp, zero, q)
    top[...] = jnp.full_like(top, -1e30)
    total[...] = jnp.zeros_like(total)
    acc[...] = jnp.zeros_like(acc)
    tile = min(TILE, half)

    def update(h, k, v, at, mask):
        scores = lax.dot_general(
            k, qpad[h, at], (((1,), (1,)), ((), ())), preferred_element_type=jnp.float32
        )
        if mask is not None:
            kpos = lax.broadcasted_iota(jnp.int32, scores.shape, 0)
            qpos = mask + lax.broadcasted_iota(jnp.int32, scores.shape, 1)
            scores = jnp.where(kpos <= qpos, scores, -1e30)
        old = top[h : h + 1, at]
        new = jnp.maximum(old, jnp.max(scores, axis=0, keepdims=True))
        p = jnp.exp(scores - new)
        factor = jnp.exp(old - new)
        top[h : h + 1, at] = new
        total[h : h + 1, at] = total[h : h + 1, at] * factor + jnp.sum(p, axis=0, keepdims=True)
        acc[h, :, at] = acc[h, :, at] * factor + lax.dot_general(
            v, p.astype(jnp.bfloat16), (((0,), (0,)), ((), ())),
            preferred_element_type=jnp.float32,
        )

    def key_value(piece, h):
        k = piece[:, h * both : (h + 1) * both]
        v = piece[:, head_cols + h * vsize : head_cols + (h + 1) * vsize]
        return k, v

    def absorb(lev, pair):
        slot = slot_of(lev, pair)
        for h in range(per):
            for which in range(2):
                piece = kvb[slot, which * half : (which + 1) * half]
                k, v = key_value(piece, h)
                for start in range(0, 2 * queries, tile):
                    update(h, k, v, slice(start, start + tile), None)

    def absorb_diag():
        for h in range(per):
            for block in range(4):
                which, pair = block // 2, block % 2
                piece = kvb[slot_of(level, pair), which * half : (which + 1) * half]
                k, v = key_value(piece, h)
                base = block * half
                for m in range(2):
                    for start in range(base, queries, tile):
                        at = slice(m * queries + start, m * queries + start + tile)
                        update(h, k, v, at, start - base if start < base + half else None)

    @pl.loop(2, level + 1)
    def _(j):
        await_pair(level - j, first)
        absorb(level - j + 1, first)

    def product(ref):
        gate = ref[:, :channels].astype(jnp.float32)
        other = ref[:, channels : 2 * channels].astype(jnp.float32)
        return (gate * other).astype(jnp.bfloat16).astype(jnp.float32)

    padded[EDGE:] = product(cbuf)

    @pl.when(s > 0)
    def _():
        tail_copy.wait_recv()
        padded[:EDGE] = product(tail)

    @pl.when(s == 0)
    def _():
        padded[:EDGE] = jnp.zeros((EDGE, channels), jnp.float32)

    count = taps_ref.shape[0]
    conv = jnp.zeros((rows, channels), jnp.float32)
    for tap in range(count):
        begin = EDGE - count + 1 + tap
        conv = conv + taps_ref[tap : tap + 1] * padded[begin : begin + rows]
    gated = cbuf[:, 2 * channels :].astype(jnp.float32) * conv
    cvout[...] = (gated * group_scale(gated, GROUP) * cgain_ref[...]).astype(jnp.bfloat16)
    load_wo.wait()

    def partial(target):
        return jnp.dot(cvout[block_at(target), :], wobuf[...], preferred_element_type=jnp.float32)

    cross_copy = remote(cross, cross_in, cross_send, cross_recv, {"tp": near})
    fin_copy = remote(fin, fin_in, fin_send, fin_recv, {"tp": near})
    far_sum = remote(far, far_in, fs_send, fs_recv, {"tp": away})
    cross[...] = partial(diag).astype(jnp.bfloat16)
    cross_copy.start()
    fin[...] = partial(near).astype(jnp.bfloat16)
    fin_copy.start()
    out_ref[...] = partial(t)
    toward = partial(away)
    cross_copy.wait_recv()
    far[...] = (toward + cross_in[...].astype(jnp.float32)).astype(jnp.bfloat16)
    far_sum.start()

    @pl.when(has_down)
    def _():
        absorb(0, first)

    absorb_diag()

    @pl.when(has_down)
    def _():
        await_pair(level - 1, second)
        absorb(level - 1, second)

    w_far.wait_recv()
    w_side.start()
    w_pass(side, 3).start()

    @pl.loop(2, level + 1)
    def _(j):
        await_pair(level - j, second)
        absorb(level - j, second)

    w_side.wait_recv()
    w_pass(1 - side, 4).start()

    for h in range(per):
        inverse = 1.0 / total[h : h + 1]
        mapped = acc[h] * inverse
        attn = mapped[:, :queries] - lam_ref[side * per + h] * mapped[:, queries:]
        scale = lax.rsqrt(jnp.mean(attn * attn, axis=0, keepdims=True) + eps)
        result = (attn * scale).T * sub_ref[...]
        obuf[:, h * vsize : (h + 1) * vsize] = result.astype(jnp.bfloat16)
        logs = top[h : h + 1] + jnp.log(total[h : h + 1])
        for m in range(2):
            low = logs[:, m * queries : m * queries + rows]
            high = logs[:, m * queries + rows : (m + 1) * queries]
            log_ref[side * per + h, m : m + 1, :] = jnp.where(side == 0, low, high)
            lout[h, m : m + 1, :] = jnp.where(side == 0, high, low)

    me8 = t * 2 + side

    def piece_rows(which, target):
        return pl.ds(pl.multiple_of(which * rows + target * own, own), own)

    def o_copy(which, target, index):
        return remote(
            obuf.at[piece_rows(which, target)], hin.at[me8], o_send.at[index], o_recv.at[me8],
            {"sp": level * 2 + which, "tp": target},
        )

    def o_wait(which, source, index):
        spot = hin.at[source * 2 + which]
        return remote(spot, spot, o_send.at[index], o_recv.at[source * 2 + which], mate_id)

    peers = [(1 - side, diag), (1 - side, away), (side, diag), (side, away)]
    peers += [(1 - side, t), (1 - side, near), (side, near)]
    for index, (which, target) in enumerate(peers):
        o_copy(which, target, index).start()
    log_copy = remote(lout, lin, log_sem.at[0], log_sem.at[1], mate_id)
    log_copy.start()
    hin[me8] = obuf[piece_rows(side, t)]
    fin_copy.wait_recv()
    far_sum.wait_recv()
    out_ref[...] += fin_in[...].astype(jnp.float32) + far_in[...].astype(jnp.float32)
    load_wa.wait()
    w_near.wait_recv()
    w_pass(side, 3).wait_recv()
    w_pass(1 - side, 4).wait_recv()
    for index, (which, source) in enumerate(peers):
        o_wait(which, source, index).wait_recv()
    lhs = jnp.concatenate([hin[i] for i in range(2 * tp)], axis=1)
    out_ref[...] += jnp.dot(lhs, wfull[...], preferred_element_type=jnp.float32)
    log_copy.wait_recv()
    for h in range(per):
        log_ref[(1 - side) * per + h] = lin[h]

    near_copy.wait_send()
    for copy in far_copies + forwards:
        copy.wait_send()
    for pair in range(2):
        give_copy(pair).wait_send()
        giveq_copy(pair).wait_send()
    for copy in (w_near, w_far, w_side, w_pass(side, 3), w_pass(1 - side, 4)):
        copy.wait_send()
    for copy in (cross_copy, fin_copy, far_sum, log_copy):
        copy.wait_send()
    for index, (which, target) in enumerate(peers):
        o_copy(which, target, index).wait_send()

    @pl.when(has_up)
    def _():
        @pl.loop(0, level + 1)
        def _(lev):
            for pair in range(2):
                for which in range(2):
                    up_copy(lev, pair, which).wait_send()

    @pl.when(s < sp - 1)
    def _():
        tail_copy.wait_send()


def vmem():
    return pl.BlockSpec(memory_space=pltpu.VMEM)


def on_device(
    inputs, norm_gain, w_query, w_key, w_value, query_gain, key_gain, lambdas, sub_gain,
    w_gate_b, w_gate_c, w_conv_in, conv_taps, conv_gain, w_out_att, w_out_conv,
):
    heads = lambdas.shape[0]
    comp = query_gain.shape[1]
    vsize = sub_gain.shape[0]
    channels = conv_gain.shape[0]
    own, width = inputs.shape
    tp = lax.axis_size("tp")
    sp = lax.axis_size("sp")
    rows = own * tp
    half = rows // 2
    qcols = heads * 2 * comp
    mine = qcols // 2
    per = heads // 2
    dma = pltpu.SemaphoreType.DMA
    bf, f32 = jnp.bfloat16, jnp.float32
    weights = (w_key, w_value, w_query, w_gate_c, w_conv_in, w_gate_b, w_out_att, w_out_conv)
    groups = sp // 2 * 4
    piece = pltpu.VMEM((own, width), bf)
    any_spec = pl.BlockSpec(memory_space=pl.ANY)
    mixed, log_sums = pl.pallas_call(
        functools.partial(layer, sp, tp, comp, heads),
        out_shape=(
            jax.ShapeDtypeStruct((own, width), f32),
            jax.ShapeDtypeStruct((heads, 2, rows), f32),
        ),
        in_specs=[vmem()] * 4 + [pl.BlockSpec(memory_space=pltpu.SMEM)] + [vmem()] * 3
        + [any_spec] * 8,
        out_specs=(vmem(), vmem()),
        scratch_shapes=[
            pltpu.VMEM((rows, width), bf),
            pltpu.VMEM((6, width, qcols), bf),
            pltpu.VMEM((tp * w_out_att.shape[0], width), bf),
            pltpu.VMEM(w_out_conv.shape, bf),
            pltpu.VMEM((8, qcols), f32),
            pltpu.VMEM((sp, 2 * half, 2 * mine), bf),
            pltpu.VMEM((2 * rows, mine), bf),
            pltpu.VMEM((2, half, 2 * mine), bf),
            pltpu.VMEM((2, half, mine), bf),
            pltpu.VMEM((per, 4 * rows, 2 * comp), bf),
            pltpu.VMEM((per, 4 * rows), f32),
            pltpu.VMEM((per, 4 * rows), f32),
            pltpu.VMEM((per, vsize, 4 * rows), f32),
            pltpu.VMEM((rows, 3 * channels), bf),
            pltpu.VMEM((EDGE, 2 * channels), bf),
            pltpu.VMEM((EDGE + rows, channels), f32),
            pltpu.VMEM((rows, channels), bf),
            piece, piece, piece, piece, piece, piece,
            pltpu.VMEM((2 * rows, per * vsize), bf),
            pltpu.VMEM((2 * tp, own, per * vsize), bf),
            pltpu.VMEM((per, 2, rows), f32),
            pltpu.VMEM((per, 2, rows), f32),
            dma((8,)), dma((2,)), dma((CHUNKS,)), dma((CHUNKS,)), dma((CHUNKS,)), dma((CHUNKS,)),
            dma((groups,)), dma((groups,)), dma((2,)), dma((2,)), dma((2,)), dma((2,)),
            dma((5,)), dma((5,)), dma(()), dma(()), dma(()), dma(()), dma(()), dma(()),
            dma((7,)), dma((2 * tp,)), dma((2,)),
        ],
        compiler_params=pltpu.CompilerParams(
            collective_id=0, has_side_effects=True, vmem_limit_bytes=VMEM_LIMIT
        ),
        name="layer",
    )(
        inputs, norm_gain[None], query_gain, key_gain, lambdas, sub_gain[None], conv_taps,
        conv_gain[None], *weights,
    )
    return (mixed, log_sums)


def solution(mesh):
    in_specs = (
        P(("sp", "tp"), None),
        P(),
        P(None, "tp"),
        P(None, "tp"),
        P(None, "tp"),
        P(),
        P(),
        P("tp"),
        P(),
        P(None, "tp"),
        P(None, "tp"),
        P(None, "tp"),
        P(None, "tp"),
        P("tp"),
        P("tp", None),
        P("tp", None),
    )
    out_specs = (P(("sp", "tp"), None), P("tp", None, "sp"))
    return jax.shard_map(
        on_device, mesh=mesh, in_specs=in_specs, out_specs=out_specs, check_vma=False
    )
```

time: 101 us -> 80.6 us (0.80)
  the two profiles are of different devices: /device:TPU:24 before, /device:TPU:25 now
where the time goes in v1:
time: 80.6 us; the launch traced here: 80.5 us
  Pallas kernels  76.9 us (95%)
  local copies, waits for them, and re-layouts  2.9 us (4%)
    pallas_call x1, Pallas kernels, on_device(): pl.pallas_call(functools.partial(layer, sp, tp, comp, heads), out_shape=(...  76.9 us
    unnamed x4, local copies, waits for them, and re-layouts  2.9 us

profile of v1, /device:TPU:25, one launch (start us, length us, event | category | flops | bytes accessed | tf_op | source)
XLA Modules:
  0.0 80.5 jit_solution(9245855271558427640)
XLA Ops:
  0.6 76.9 %layer.1 = (f32[128,2048]{1,0:T(8,128)}, f32[2,2,512]{2,1,0:T(2,128)}) custom-call(bf16[128,2048]{1,0:T(8,128)(2,1)} %x_ref.1, f32[1,2048]{1,0:T(1,128)} %bitcast.3, f32[2,64]{1,0:T(2,128)} %qg_ref.1, f32[2,64]{1,0:T(2,128)} %kg_ref.1, f32[2]{0:T(128)} %lam_ref.1, f32[1,128]{1,0:T(1,128)} %bitcast.5, f32[3,256]{1,0:T(4,128)} %taps_ref.1, f32[1,256]{1,0:T(1,128)} %bitcast.4, ...), custom_call_target="tpu_custom_call" | custom-call | tf_op jit(solution)/shard_map/layer/pallas_call | solution.py:531
  77.6 0.0 copy-start
  77.6 2.3 %copy.20 = f32[128,2048]{1,0:T(8,128)} copy(f32[128,2048]{1,0:T(8,128)} %get-tuple-element.4) | data formatting | bytes 2097152
  79.9 0.0 copy-done
  79.9 0.6 copy.21
Async XLA Ops:
  77.6 2.3 %copy-start = (f32[2,2,512]{2,1,0:T(2,128)S(1)}, f32[2,2,512]{2,1,0:T(2,128)}, u32[]{:S(2)}) copy-start(f32[2,2,512]{2,1,0:T(2,128)} %get-tuple-element.5) | copy-start | bytes 24580

commit v2 on v1

--- a/solution.py
+++ b/solution.py
@@ -13,7 +13,7 @@
 VMEM_LIMIT = 62 * 1024 * 1024
 CHUNKS = 4
 EDGE = 16
-TILE = 256
+TILE = 128
 
 
 def rms_scale(values):
@@ -50,7 +50,7 @@
     x_ref, gain_ref, qg_ref, kg_ref, lam_ref, sub_ref, taps_ref, cgain_ref,
     wk, wv, wq, wc, wi, wb, wa, wo,
     out_ref, log_ref,
-    held, wbuf, wfull, wobuf, gains, kvb, qb, give_kv, give_q, qpad, top, total, acc, cbuf, tail,
+    held, wbuf, wfull, wobuf, gains, kvb, vt, qb, give_kv, give_q, qpad, top, total, acc, cbuf, tail,
     padded, cvout, cross, fin, far, cross_in, fin_in, far_in, obuf, hin, lout, lin,
     wsem, near_sem, far_send, far_recv, fwd_send, fwd_recv, up_send, kv_recv, gk_send, gq_send,
     q_recv, tail_sem, w_send, w_recv, cross_send, cross_recv, fin_send, fin_recv, fs_send, fs_recv,
@@ -102,6 +102,7 @@
     def block_at(index):
         return pl.ds(pl.multiple_of(index * own, own), own)
 
+    phase("norm")
     x = x_ref[...].astype(jnp.float32)
     held[block_at(t), :] = (rms_scale(x) * gain_ref[...]).astype(jnp.bfloat16)
     for row, ref in ((0, kg_ref), (1, qg_ref)):
@@ -110,6 +111,7 @@
                 at = (h * 2 + m) * comp
                 gains[row : row + 1, at : at + comp] = ref[m : m + 1, :]
 
+    phase("barrier")
     barrier = pltpu.get_barrier_semaphore()
 
     def hello(where):
@@ -138,6 +140,7 @@
 
     pl.semaphore_wait(barrier, 7 + ups + downs + side * ups + (1 - side) * downs)
 
+    phase("defs")
     part = own // CHUNKS
 
     def chunk_at(index, c):
@@ -260,30 +263,47 @@
         await_group(lev, pair, side)
         await_group(lev, pair, 1 - side)
 
+    phase("wait_kv_weights")
     loads[0].wait()
     loads[1].wait()
+    phase("wait_near")
     near_copy.wait_recv()
+    phase("kv_first")
     project_kv(first)
     w_near.start()
-    w_far.start()
+    phase("q_first")
     loads[2].wait()
     project_q(first)
+    phase("conv_first")
     for load in loads[3:]:
         load.wait()
     project_conv(first)
+    phase("mate_first")
     await_group(level, first, 1 - side)
 
+    phase("below_first")
     @pl.when(has_down)
     def _():
         await_pair(level - 1, first)
 
+    phase("far_wait")
     for c in range(CHUNKS):
         far_copies[c].wait_recv()
         forwards[c].start()
+    w_far.start()
     for copy in forwards:
         copy.wait_recv()
+    phase("kv_second")
     project_kv(second)
+    phase("q_second")
     project_q(second)
+    phase("below_first2")
+
+    @pl.when(level > 1)
+    def _():
+        await_pair(level - 2, first)
+
+    phase("conv_second")
     project_conv(second)
 
     tail_copy = remote(
@@ -295,10 +315,12 @@
     def _():
         tail_copy.start()
 
+    phase("mate_second")
     await_group(level, second, 1 - side)
     giveq_copy(0).wait_recv()
     giveq_copy(1).wait_recv()
 
+    phase("qpad")
     queries = 2 * rows
     lane = lax.broadcasted_iota(jnp.int32, (queries, both), 1)
     for h in range(per):
@@ -311,56 +333,89 @@
     acc[...] = jnp.zeros_like(acc)
     tile = min(TILE, half)
 
-    def update(h, k, v, at, mask):
-        scores = lax.dot_general(
-            k, qpad[h, at], (((1,), (1,)), ((), ())), preferred_element_type=jnp.float32
-        )
-        if mask is not None:
-            kpos = lax.broadcasted_iota(jnp.int32, scores.shape, 0)
-            qpos = mask + lax.broadcasted_iota(jnp.int32, scores.shape, 1)
-            scores = jnp.where(kpos <= qpos, scores, -1e30)
-        old = top[h : h + 1, at]
-        new = jnp.maximum(old, jnp.max(scores, axis=0, keepdims=True))
-        p = jnp.exp(scores - new)
-        factor = jnp.exp(old - new)
-        top[h : h + 1, at] = new
-        total[h : h + 1, at] = total[h : h + 1, at] * factor + jnp.sum(p, axis=0, keepdims=True)
-        acc[h, :, at] = acc[h, :, at] * factor + lax.dot_general(
-            v, p.astype(jnp.bfloat16), (((0,), (0,)), ((), ())),
-            preferred_element_type=jnp.float32,
-        )
-
-    def key_value(piece, h):
-        k = piece[:, h * both : (h + 1) * both]
-        v = piece[:, head_cols + h * vsize : head_cols + (h + 1) * vsize]
-        return k, v
+    def run_tiles(work):
+        def score(item):
+            h, keys, values, at, mask = item
+            return lax.dot_general(
+                keys(), qpad[h, at], (((1,), (1,)), ((), ())), preferred_element_type=jnp.float32
+            )
+
+        ahead = score(work[0])
+        for index, (h, keys, values, at, mask) in enumerate(work):
+            scores = ahead
+            if index + 1 < len(work):
+                ahead = score(work[index + 1])
+            if mask is not None:
+                kpos = lax.broadcasted_iota(jnp.int32, scores.shape, 0)
+                qpos = mask + lax.broadcasted_iota(jnp.int32, scores.shape, 1)
+                scores = jnp.where(kpos <= qpos, scores, -1e30)
+            old = top[h : h + 1, at]
+            new = jnp.maximum(old, jnp.max(scores, axis=0, keepdims=True))
+            p = jnp.exp(scores - new)
+            factor = jnp.exp(old - new)
+            top[h : h + 1, at] = new
+            total[h : h + 1, at] = total[h : h + 1, at] * factor + jnp.sum(
+                p, axis=0, keepdims=True
+            )
+            acc[h, :, at] = acc[h, :, at] * factor + jnp.dot(
+                values(), p.astype(jnp.bfloat16), preferred_element_type=jnp.float32
+            )
+
+    def key_part(slot, h, begin, size):
+        return lambda: kvb[slot, begin : begin + size, h * both : (h + 1) * both]
+
+    def value_part(which, h, begin, size):
+        return lambda: vt[which, h, :, begin : begin + size]
+
+    def turn_values(slot, which):
+        for h in range(per):
+            cols = slice(head_cols + h * vsize, head_cols + (h + 1) * vsize)
+            vt[which, h] = kvb[slot, :, cols].T
 
     def absorb(lev, pair):
         slot = slot_of(lev, pair)
-        for h in range(per):
-            for which in range(2):
-                piece = kvb[slot, which * half : (which + 1) * half]
-                k, v = key_value(piece, h)
-                for start in range(0, 2 * queries, tile):
-                    update(h, k, v, slice(start, start + tile), None)
+        turn_values(slot, 0)
+        run_tiles(
+            [
+                (
+                    h, key_part(slot, h, which * half, half),
+                    value_part(0, h, which * half, half), slice(start, start + tile), None,
+                )
+                for h in range(per)
+                for start in range(0, 2 * queries, tile)
+                for which in range(2)
+            ]
+        )
 
     def absorb_diag():
+        work = []
+        for pair in range(2):
+            turn_values(slot_of(level, pair), pair)
         for h in range(per):
             for block in range(4):
                 which, pair = block // 2, block % 2
-                piece = kvb[slot_of(level, pair), which * half : (which + 1) * half]
-                k, v = key_value(piece, h)
                 base = block * half
                 for m in range(2):
                     for start in range(base, queries, tile):
                         at = slice(m * queries + start, m * queries + start + tile)
-                        update(h, k, v, at, start - base if start < base + half else None)
-
-    @pl.loop(2, level + 1)
-    def _(j):
-        await_pair(level - j, first)
-        absorb(level - j + 1, first)
-
+                        inside = start < base + half
+                        size = min(start - base + tile, half) if inside else half
+                        work.append(
+                            (
+                                h, key_part(slot_of(level, pair), h, which * half, size),
+                                value_part(pair, h, which * half, size), at,
+                                start - base if inside else None,
+                            )
+                        )
+        run_tiles(work)
+
+    phase("absorb1")
+
+    @pl.when(has_down)
+    def _():
+        absorb(level - 1, first)
+
+    phase("conv")
     def product(ref):
         gate = ref[:, :channels].astype(jnp.float32)
         other = ref[:, channels : 2 * channels].astype(jnp.float32)
@@ -392,6 +447,7 @@
     cross_copy = remote(cross, cross_in, cross_send, cross_recv, {"tp": near})
     fin_copy = remote(fin, fin_in, fin_send, fin_recv, {"tp": near})
     far_sum = remote(far, far_in, fs_send, fs_recv, {"tp": away})
+    phase("partial")
     cross[...] = partial(diag).astype(jnp.bfloat16)
     cross_copy.start()
     fin[...] = partial(near).astype(jnp.bfloat16)
@@ -402,29 +458,45 @@
     far[...] = (toward + cross_in[...].astype(jnp.float32)).astype(jnp.bfloat16)
     far_sum.start()
 
-    @pl.when(has_down)
-    def _():
-        absorb(0, first)
-
-    absorb_diag()
-
-    @pl.when(has_down)
-    def _():
-        await_pair(level - 1, second)
-        absorb(level - 1, second)
-
+    phase("w_far")
     w_far.wait_recv()
     w_side.start()
     w_pass(side, 3).start()
-
+    phase("near_loop")
+
+    @pl.loop(3, level + 1)
+    def _(j):
+        await_pair(level - j, first)
+        absorb(level - j + 1, first)
+
+    @pl.when(level > 1)
+    def _():
+        absorb(0, first)
+
+    phase("below_second")
+
+    @pl.when(has_down)
+    def _():
+        await_pair(level - 1, second)
+
+    phase("diag")
+    absorb_diag()
+
+    @pl.when(has_down)
+    def _():
+        absorb(level - 1, second)
+
+    phase("far_loop")
     @pl.loop(2, level + 1)
     def _(j):
         await_pair(level - j, second)
         absorb(level - j, second)
 
+    phase("w_side")
     w_side.wait_recv()
     w_pass(1 - side, 4).start()
 
+    phase("finalize")
     for h in range(per):
         inverse = 1.0 / total[h : h + 1]
         mapped = acc[h] * inverse
@@ -439,6 +511,7 @@
             log_ref[side * per + h, m : m + 1, :] = jnp.where(side == 0, low, high)
             lout[h, m : m + 1, :] = jnp.where(side == 0, high, low)
 
+    phase("send_o")
     me8 = t * 2 + side
 
     def piece_rows(which, target):
@@ -461,21 +534,27 @@
     log_copy = remote(lout, lin, log_sem.at[0], log_sem.at[1], mate_id)
     log_copy.start()
     hin[me8] = obuf[piece_rows(side, t)]
+    phase("conv_sum")
     fin_copy.wait_recv()
     far_sum.wait_recv()
     out_ref[...] += fin_in[...].astype(jnp.float32) + far_in[...].astype(jnp.float32)
+    phase("w_wait")
     load_wa.wait()
     w_near.wait_recv()
     w_pass(side, 3).wait_recv()
     w_pass(1 - side, 4).wait_recv()
+    phase("o_wait")
     for index, (which, source) in enumerate(peers):
         o_wait(which, source, index).wait_recv()
+    phase("last_dot")
     lhs = jnp.concatenate([hin[i] for i in range(2 * tp)], axis=1)
     out_ref[...] += jnp.dot(lhs, wfull[...], preferred_element_type=jnp.float32)
+    phase("log")
     log_copy.wait_recv()
     for h in range(per):
         log_ref[(1 - side) * per + h] = lin[h]
 
+    phase("sends")
     near_copy.wait_send()
     for copy in far_copies + forwards:
         copy.wait_send()
@@ -500,6 +579,12 @@
     @pl.when(s < sp - 1)
     def _():
         tail_copy.wait_send()
+
+    phase(None)
+
+
+def phase(name):
+    pass
 
 
 def vmem():
@@ -544,6 +629,7 @@
             pltpu.VMEM(w_out_conv.shape, bf),
             pltpu.VMEM((8, qcols), f32),
             pltpu.VMEM((sp, 2 * half, 2 * mine), bf),
+            pltpu.VMEM((2, per, vsize, 2 * half), bf),
             pltpu.VMEM((2 * rows, mine), bf),
             pltpu.VMEM((2, half, 2 * mine), bf),
             pltpu.VMEM((2, half, mine), bf),

time: 80.6 us -> 57.8 us (0.72)
  Pallas kernels: 76.9 us -> 54.1 us
    pallas_call x1, Pallas kernels: 76.9 us -> 54.1 us  [on_device(): pl.pallas_call(functools.partial(layer, sp, tp, comp, heads), out_shape=(...]
where the time goes in v2:
time: 57.8 us; the launch traced here: 57.7 us
  Pallas kernels  54.1 us (94%)
  local copies, waits for them, and re-layouts  2.9 us (5%)
  between operations  0.65 us (1%)
    pallas_call x1, Pallas kernels, on_device(): pl.pallas_call(functools.partial(layer, sp, tp, comp, heads), out_shape=(...  54.1 us
    unnamed x4, local copies, waits for them, and re-layouts  2.9 us

profile of v2, /device:TPU:25, one launch (start us, length us, event | category | flops | bytes accessed | tf_op | source)
XLA Modules:
  0.0 57.7 jit_solution(18146319261912918787)
XLA Ops:
  0.6 54.1 %layer.1 = (f32[128,2048]{1,0:T(8,128)}, f32[2,2,512]{2,1,0:T(2,128)}) custom-call(bf16[128,2048]{1,0:T(8,128)(2,1)} %x_ref.1, f32[1,2048]{1,0:T(1,128)} %bitcast.3, f32[2,64]{1,0:T(2,128)} %qg_ref.1, f32[2,64]{1,0:T(2,128)} %kg_ref.1, f32[2]{0:T(128)} %lam_ref.1, f32[1,128]{1,0:T(1,128)} %bitcast.5, f32[3,256]{1,0:T(4,128)} %taps_ref.1, f32[1,256]{1,0:T(1,128)} %bitcast.4, ...), custom_call_target="tpu_custom_call" | custom-call | tf_op jit(solution)/shard_map/layer/pallas_call | solution.py:616
  54.7 0.0 copy-start
  54.8 2.3 %copy.20 = f32[128,2048]{1,0:T(8,128)} copy(f32[128,2048]{1,0:T(8,128)} %get-tuple-element.4) | data formatting | bytes 2097152
  57.1 0.0 copy-done
  57.1 0.6 %copy.21 = f32[2,2,512]{2,1,0:T(2,128)} copy(f32[2,2,512]{2,1,0:T(2,128)S(1)} %copy-done) | data formatting | bytes 16384
Async XLA Ops:
  54.7 2.3 %copy-start = (f32[2,2,512]{2,1,0:T(2,128)S(1)}, f32[2,2,512]{2,1,0:T(2,128)}, u32[]{:S(2)}) copy-start(f32[2,2,512]{2,1,0:T(2,128)} %get-tuple-element.5) | copy-start | bytes 24580

commit v3 on v2

v3 whole, which is shorter than its diff:
```python
import functools

import jax
import jax.numpy as jnp
from jax import lax
from jax.experimental import pallas as pl
from jax.experimental.pallas import tpu as pltpu
from jax.sharding import PartitionSpec as P

GROUP = 64
eps = 1e-06
MESH = pl.DeviceIdType.MESH
VMEM_LIMIT = 62 * 1024 * 1024
CHUNKS = 4
EDGE = 16
TILE = 128
DEPTH = 2
W_PARTS = 2


def rms_scale(values):
    return values * lax.rsqrt(jnp.mean(values * values, axis=-1, keepdims=True) + eps)


def flip(index, bit):
    return index + bit - 2 * bit * lax.rem(index // bit, 2)


def remote(src, dst, send, recv, where):
    return pltpu.make_async_remote_copy(
        src_ref=src, dst_ref=dst, send_sem=send, recv_sem=recv, device_id=where,
        device_id_type=MESH,
    )


def group_scale(values, size):
    lanes = values.shape[1]
    row = lax.broadcasted_iota(jnp.int32, (lanes, lanes), 0) // size
    col = lax.broadcasted_iota(jnp.int32, (lanes, lanes), 1) // size
    ones = jnp.where(row == col, 1.0, 0.0).astype(jnp.bfloat16)
    squares = values * values
    high = squares.astype(jnp.bfloat16)
    low = (squares - high.astype(jnp.float32)).astype(jnp.bfloat16)
    sums = jnp.dot(high, ones, preferred_element_type=jnp.float32) + jnp.dot(
        low, ones, preferred_element_type=jnp.float32
    )
    return lax.rsqrt(sums * (1.0 / size) + eps)


def layer(
    sp, tp, comp, heads,
    x_ref, gain_ref, qg_ref, kg_ref, lam_ref, sub_ref, taps_ref, cgain_ref,
    wk, wv, wq, wc, wi, wb, wa, wo,
    out_ref, log_ref,
    held, wbuf, wfull, wobuf, gains, kvb, vt, qb, give_kv, give_q, qpad, top, total, acc, cbuf, tail,
    padded, cvout, lamb, cross, fin, far, cross_in, fin_in, far_in, obuf, hin, lout, lin,
    wsem, near_sem, far_send, far_recv, fwd_send, fwd_recv, up_send, kv_recv, gk_send, gq_send,
    q_recv, tail_sem, w_send, w_recv, cross_send, cross_recv, fin_send, fin_recv, fs_send, fs_recv,
    o_send, o_recv, log_send, log_recv, lam_sem, qs_send, qs_recv,
):
    s = lax.axis_index("sp")
    t = lax.axis_index("tp")
    level, side = s // 2, lax.rem(s, 2)
    levels = sp // 2
    mate = level * 2 + 1 - side
    near, away = flip(t, 1), flip(t, 2)
    diag = flip(near, 2)
    first, second = t // 2, 1 - t // 2
    own = x_ref.shape[0]
    rows = own * tp
    half = rows // 2
    head_cols = heads * 2 * comp // 2
    per = heads // 2
    vsize = sub_ref.shape[1]
    both = 2 * comp
    channels = cgain_ref.shape[1]
    has_up, has_down = level < levels - 1, level > 0

    def as_int(flag):
        return flag.astype(jnp.int32)

    ups, downs = as_int(has_up), as_int(has_down)
    mate_id = {"sp": mate}
    odd = lax.rem(t, 2)
    is_top, is_low = as_int(level == levels - 1), as_int(level == levels - 2)
    high_pair = is_top + is_low
    swapped = is_low * odd + is_top * (1 - odd)
    swaps = swapped == 1
    aside = is_low * (1 - odd) + is_top
    job_level = level + is_low * odd - is_top * (1 - odd)
    job_tp = t + swapped * (near - t)
    cross_sp = s + 2 * is_low - 2 * is_top
    cross_id = {"sp": cross_sp, "tp": near}
    up_id = {
        "sp": s + (1 - is_top) * (2 - 2 * is_low * (1 - odd)) - 2 * is_top * (1 - odd),
        "tp": t + aside * (near - t),
    }
    sends_own = is_top * odd == 0
    relays = is_top * (1 - odd) == 0
    groups = sp // 2 * 4

    loads = [
        pltpu.make_async_copy(w, wbuf.at[i], wsem.at[i])
        for i, w in enumerate((wk, wv, wq, wc, wi, wb))
    ]
    for load in loads:
        load.start()
    wa_rows = wa.shape[0]
    half_rows = wa_rows // 2

    def shard(index):
        return pl.ds(pl.multiple_of(index * wa_rows, wa_rows), wa_rows)

    w_part = half_rows // W_PARTS

    def part_of(index, which, c):
        begin = index * wa_rows + which * half_rows + c * w_part
        return pl.ds(pl.multiple_of(begin, w_part), w_part)

    load_wa = pltpu.make_async_copy(wa, wfull.at[shard(t)], wsem.at[6])
    load_wo = pltpu.make_async_copy(wo, wobuf, wsem.at[7])
    load_wa.start()
    load_wo.start()

    def block_at(index):
        return pl.ds(pl.multiple_of(index * own, own), own)

    phase("norm")
    x = x_ref[...].astype(jnp.float32)
    held[block_at(t), :] = (rms_scale(x) * gain_ref[...]).astype(jnp.bfloat16)
    for row, ref in ((0, kg_ref), (1, qg_ref)):
        for h in range(heads):
            for m in range(2):
                at = (h * 2 + m) * comp
                gains[row : row + 1, at : at + comp] = ref[m : m + 1, :]

    phase("barrier")
    barrier = pltpu.get_barrier_semaphore()

    def hello(where):
        pl.semaphore_signal(barrier, inc=1, device_id=where, device_id_type=MESH)

    for peer in (near, away, diag):
        hello({"tp": peer})
    for peer in (t, near, away, diag):
        hello({"sp": mate, "tp": peer})

    plain_up = level < levels - 2
    plain_down = has_down & (level < levels - 1)

    @pl.when(plain_up)
    def _():
        hello({"sp": s + 2})

    @pl.when(plain_down)
    def _():
        hello({"sp": s - 2})

    @pl.when(high_pair == 1)
    def _():
        for which in range(2):
            for peer in range(tp):
                hello({"sp": (cross_sp // 2) * 2 + which, "tp": peer})

    @pl.when((side == 1) & has_up)
    def _():
        hello({"sp": s + 1})

    @pl.when((side == 0) & has_down)
    def _():
        hello({"sp": s - 1})

    expected = 7 + as_int(plain_up) + as_int(plain_down) + 2 * tp * high_pair
    pl.semaphore_wait(barrier, expected + side * ups + (1 - side) * downs)

    phase("defs")
    part = own // CHUNKS

    def chunk_at(index, c):
        return pl.ds(pl.multiple_of(index * own + c * part, part), part)

    def far_copy(c):
        spot = held.at[chunk_at(t, c)]
        return remote(spot, spot, far_send.at[c], far_recv.at[c], {"tp": away})

    def forward(c):
        spot = held.at[chunk_at(away, c)]
        return remote(spot, spot, fwd_send.at[c], fwd_recv.at[c], {"tp": near})

    far_copies = [far_copy(c) for c in range(CHUNKS)]
    forwards = [forward(c) for c in range(CHUNKS)]
    mine = held.at[block_at(t)]
    near_copy = remote(mine, mine, near_sem.at[0], near_sem.at[1], {"tp": near})
    near_copy.start()
    for copy in far_copies:
        copy.start()
    for h in range(heads):
        lamb[0, h] = jnp.full(lamb.shape[2:], lam_ref[h], jnp.float32)
    lam_copy = remote(lamb.at[0], lamb.at[1], lam_sem.at[0], lam_sem.at[1], {"tp": near})
    lam_copy.start()

    w_near = remote(wa, wfull.at[shard(t)], w_send.at[0], w_recv.at[0], {"tp": near})
    def w_far(c):
        return remote(
            wa.at[pl.ds(pl.multiple_of(side * half_rows + c * w_part, w_part), w_part)],
            wfull.at[part_of(t, side, c)], w_send.at[1 + c], w_recv.at[1 + c], {"tp": away},
        )

    def w_side(c):
        spot = wfull.at[part_of(away, side, c)]
        return remote(spot, spot, w_send.at[3 + c], w_recv.at[3 + c], mate_id)

    def w_pass(which, kind, c):
        spot = wfull.at[part_of(away, which, c)]
        slot = 5 + 2 * kind + c
        return remote(spot, spot, w_send.at[slot], w_recv.at[slot], {"tp": near})

    def w_spread(c):
        w_far(c).wait_recv()
        w_side(c).start()
        w_pass(side, 0, c).start()

    def slot_of(lev, pair):
        return lev * 2 + pair

    def group_of(lev, pair, which):
        return (lev * 2 + pair) * 2 + which

    def side_rows(which):
        return pl.ds(pl.multiple_of(which * half, half), half)

    def up_copy(lev, pair, which):
        g = group_of(lev, pair, which)
        return remote(
            kvb.at[0, slot_of(lev, pair), side_rows(which)],
            kvb.at[aside, slot_of(lev, pair), side_rows(which)],
            up_send.at[g], kv_recv.at[aside * groups + g], up_id,
        )

    def arrived(where, lev, pair, which):
        spot = kvb.at[where, slot_of(lev, pair), side_rows(which)]
        g = group_of(lev, pair, which)
        remote(spot, spot, up_send.at[g], kv_recv.at[where * groups + g], up_id).wait_recv()

    def give_copy(pair):
        return remote(
            give_kv.at[pair], kvb.at[0, slot_of(level, pair), side_rows(side)],
            gk_send.at[pair], kv_recv.at[group_of(level, pair, side)], mate_id,
        )

    def q_rows(which, pair):
        return pl.ds(pl.multiple_of(which * rows + pair * half, half), half)

    def giveq_copy(pair):
        return remote(
            give_q.at[pair], qb.at[0, q_rows(side, pair)], gq_send.at[pair], q_recv.at[pair],
            mate_id,
        )

    def swap_q(which, pair):
        index = which * 2 + pair
        return remote(
            qb.at[0, q_rows(which, pair)], qb.at[1, q_rows(which, pair)],
            qs_send.at[index], qs_recv.at[index], cross_id,
        )

    def pass_q(which, pair):
        @pl.when(swaps)
        def _():
            swap_q(which, pair).start()

    def split(values):
        low, high = values[:, :head_cols], values[:, head_cols:]
        return jnp.where(side == 0, low, high), jnp.where(side == 0, high, low)

    def pair_rows(pair):
        return pl.ds(pl.multiple_of(pair * half, half), half)

    def scaled(block, i, gain_row, factor):
        res = jnp.dot(block, wbuf[i], preferred_element_type=jnp.float32).astype(jnp.bfloat16)
        wide = res.astype(jnp.float32)
        return (wide * group_scale(wide, comp) * (gains[gain_row : gain_row + 1] * factor)).astype(
            jnp.bfloat16
        )

    def project_kv(pair):
        block = held[pair_rows(pair)]
        slot = slot_of(level, pair)
        for i in range(2):
            if i == 0:
                res = scaled(block, 0, 0, 1.0)
            else:
                res = jnp.dot(block, wbuf[1], preferred_element_type=jnp.float32).astype(
                    jnp.bfloat16
                )
            keep, give = split(res)
            cols = slice(i * head_cols, (i + 1) * head_cols)
            kvb[0, slot, side_rows(side), cols] = keep
            give_kv[pair, :, cols] = give

        give_copy(pair).start()

        @pl.when(sends_own)
        def _():
            up_copy(level, pair, side).start()

    def project_q(pair):
        block = held[pair_rows(pair)]
        keep, give = split(scaled(block, 2, 1, comp ** (-0.5)))
        qb[0, q_rows(side, pair)] = keep
        give_q[pair] = give
        giveq_copy(pair).start()
        pass_q(side, pair)

    def project_conv(pair):
        block = held[pair_rows(pair)]
        for i in range(3):
            cbuf[pair_rows(pair), i * channels : (i + 1) * channels] = jnp.dot(
                block, wbuf[3 + i], preferred_element_type=jnp.float32
            ).astype(jnp.bfloat16)

    def await_mate(pair):
        arrived(0, level, pair, 1 - side)

        @pl.when(sends_own)
        def _():
            up_copy(level, pair, 1 - side).start()

    def relay(j, pair):
        for which in (side, 1 - side):
            arrived(0, level - j, pair, which)
            up_copy(level - j, pair, which).start()

    queries = 2 * rows
    tile = min(TILE, half)

    def prepare(phase_index, pair):
        for which in range(2):
            @pl.when(swaps)
            def _():
                swap_q(which, pair).wait_recv()

            lane = lax.broadcasted_iota(jnp.int32, (half, both), 1)
            for h in range(per):
                q = qb[swapped, q_rows(which, pair), h * both : (h + 1) * both]
                zero = jnp.zeros_like(q)
                at = phase_index * rows + which * half
                qpad[h, at : at + half] = jnp.where(lane < comp, q, zero)
                qpad[h, queries + at : queries + at + half] = jnp.where(lane < comp, zero, q)

    def run_tiles(work):
        def score(item):
            h, keys, values, at, mask = item
            return lax.dot_general(
                keys(), qpad[h, at], (((1,), (1,)), ((), ())), preferred_element_type=jnp.float32
            )

        def finish(item):
            h, values, at, p, factor = item
            acc[h, :, at] = acc[h, :, at] * factor + jnp.dot(
                values(), p, preferred_element_type=jnp.float32
            )

        ahead = [score(item) for item in work[:DEPTH]]
        late = None
        for index, (h, keys, values, at, mask) in enumerate(work):
            scores = ahead.pop(0)
            if index + DEPTH < len(work):
                ahead.append(score(work[index + DEPTH]))
            if mask is not None:
                kpos = lax.broadcasted_iota(jnp.int32, scores.shape, 0)
                qpos = mask + lax.broadcasted_iota(jnp.int32, scores.shape, 1)
                scores = jnp.where(kpos <= qpos, scores, -1e30)
            old = top[h : h + 1, at]
            new = jnp.maximum(old, jnp.max(scores, axis=0, keepdims=True))
            p = jnp.exp(scores - new)
            factor = jnp.exp(old - new)
            top[h : h + 1, at] = new
            total[h : h + 1, at] = total[h : h + 1, at] * factor + jnp.sum(
                p, axis=0, keepdims=True
            )
            if late is not None:
                finish(late)
            late = (h, values, at, p.astype(jnp.bfloat16), factor)
        finish(late)

    def key_part(slot, h, begin, size):
        return lambda: kvb[swapped, slot, begin : begin + size, h * both : (h + 1) * both]

    def value_part(where, h, begin, size):
        return lambda: vt[where, h, :, begin : begin + size]

    def turn_values(slot, where):
        for h in range(per):
            cols = slice(head_cols + h * vsize, head_cols + (h + 1) * vsize)
            vt[where, h] = kvb[swapped, slot, :, cols].T

    def taken(lev, pair):
        @pl.when(swaps)
        def _():
            for which in range(2):
                arrived(1, lev, pair, which)

    def absorb(j, pair, phases):
        lev = job_level - j
        if 0 in phases:
            taken(lev, pair)
        slot = slot_of(lev, pair)
        turn_values(slot, 0)
        run_tiles(
            [
                (
                    h, key_part(slot, h, which * half, half),
                    value_part(0, h, which * half, half), slice(start, start + tile), None,
                )
                for h in range(per)
                for ph in phases
                for m in range(2)
                for start in range(
                    m * queries + ph * rows, m * queries + (ph + 1) * rows, tile
                )
                for which in range(2)
            ]
        )

    pairs = (first, second)

    def diag_work(blocks):
        work = []
        for h in range(per):
            for q_ph, q_side, k_ph, k_side in blocks:
                same = q_ph == k_ph and q_side == k_side
                slot = slot_of(job_level, pairs[k_ph])
                for m in range(2):
                    base = m * queries + q_ph * rows + q_side * half
                    for offset in range(0, half, tile):
                        size = offset + tile if same else half
                        work.append(
                            (
                                h, key_part(slot, h, k_side * half, size),
                                value_part(1 + k_ph, h, k_side * half, size),
                                slice(base + offset, base + offset + tile),
                                offset if same else None,
                            )
                        )
        return work

    def diag_ready(ph):
        taken(job_level, pairs[ph])
        turn_values(slot_of(job_level, pairs[ph]), 1 + ph)

    phase("wait_kv_weights")
    loads[0].wait()
    loads[1].wait()
    phase("wait_near")
    near_copy.wait_recv()
    phase("kv_first")
    project_kv(first)
    w_near.start()
    phase("q_first")
    loads[2].wait()
    project_q(first)
    phase("conv_first")
    for load in loads[3:]:
        load.wait()
    project_conv(first)
    tail_copy = remote(
        cbuf.at[pl.ds(rows - EDGE, EDGE), pl.ds(0, 2 * channels)], tail,
        tail_sem.at[0], tail_sem.at[1], {"sp": jnp.minimum(s + 1, sp - 1)},
    )

    @pl.when((s < sp - 1) & (first == 1))
    def _():
        tail_copy.start()

    phase("mate_first")
    await_mate(first)

    phase("below_first")
    @pl.when(has_down & relays)
    def _():
        relay(1, first)

    giveq_copy(first).wait_recv()
    pass_q(1 - side, first)
    phase("early")
    top[...] = jnp.full_like(top, -1e30)
    total[...] = jnp.zeros_like(total)
    acc[...] = jnp.zeros_like(acc)

    def early():
        prepare(0, first)
        diag_ready(0)
        run_tiles(diag_work([(0, 0, 0, 0), (0, 1, 0, 0), (0, 1, 0, 1)]))

    for c in range(CHUNKS - 1):
        far_copies[c].wait_recv()
        forwards[c].start()

    @pl.when(jnp.logical_not(swaps))
    def _():
        early()

    phase("far_wait")
    far_copies[CHUNKS - 1].wait_recv()
    forwards[CHUNKS - 1].start()
    for c in range(W_PARTS):
        w_far(c).start()
    for copy in forwards:
        copy.wait_recv()
    phase("kv_second")
    project_kv(second)
    phase("q_second")
    project_q(second)
    phase("below_first2")

    @pl.when((level > 1) & relays)
    def _():
        relay(2, first)

    phase("conv_second")
    project_conv(second)

    @pl.when((s < sp - 1) & (first == 0))
    def _():
        tail_copy.start()

    phase("early2")

    @pl.when(swaps)
    def _():
        early()

    @pl.when(relays)
    def _():
        @pl.loop(1, jnp.minimum(job_level, 2) + 1)
        def _(j):
            absorb(j, first, (0,))

    phase("mate_second")
    await_mate(second)

    phase("qpad")
    giveq_copy(second).wait_recv()
    pass_q(1 - side, second)
    phase("w_first")
    w_spread(0)
    phase("conv")
    def product(ref):
        gate = ref[:, :channels].astype(jnp.float32)
        other = ref[:, channels : 2 * channels].astype(jnp.float32)
        return (gate * other).astype(jnp.bfloat16).astype(jnp.float32)

    padded[EDGE:] = product(cbuf)

    @pl.when(s > 0)
    def _():
        tail_copy.wait_recv()
        padded[:EDGE] = product(tail)

    @pl.when(s == 0)
    def _():
        padded[:EDGE] = jnp.zeros((EDGE, channels), jnp.float32)

    count = taps_ref.shape[0]
    conv = jnp.zeros((rows, channels), jnp.float32)
    for tap in range(count):
        begin = EDGE - count + 1 + tap
        conv = conv + taps_ref[tap : tap + 1] * padded[begin : begin + rows]
    gated = cbuf[:, 2 * channels :].astype(jnp.float32) * conv
    cvout[...] = (gated * group_scale(gated, GROUP) * cgain_ref[...]).astype(jnp.bfloat16)
    load_wo.wait()

    def partial(target):
        return jnp.dot(cvout[block_at(target), :], wobuf[...], preferred_element_type=jnp.float32)

    cross_copy = remote(cross, cross_in, cross_send, cross_recv, {"tp": near})
    fin_copy = remote(fin, fin_in, fin_send, fin_recv, {"tp": near})
    far_sum = remote(far, far_in, fs_send, fs_recv, {"tp": away})
    phase("partial")
    cross[...] = partial(diag).astype(jnp.bfloat16)
    cross_copy.start()
    fin[...] = partial(near).astype(jnp.bfloat16)
    fin_copy.start()
    out_ref[...] = partial(t)
    phase("relay_second")

    @pl.when(has_down & relays)
    def _():
        relay(1, second)

    phase("toward")
    toward = partial(away)
    cross_copy.wait_recv()
    far[...] = (toward + cross_in[...].astype(jnp.float32)).astype(jnp.bfloat16)
    far_sum.start()
    phase("w_far")
    w_spread(1)
    phase("q_late")
    prepare(1, second)
    phase("near_loop")

    @pl.loop(1, job_level + 1)
    def _(j):
        @pl.when((j > 1) & (j < level) & relays)
        def _():
            relay(j + 1, first)

        @pl.when((j == job_level) & (level > 1) & (is_top == 0))
        def _():
            relay(2, second)

        @pl.when((j > 2) | jnp.logical_not(relays))
        def _():
            absorb(j, first, (0,))

        absorb(j, first, (1,))

    phase("diag")
    diag_ready(1)
    run_tiles(
        diag_work([(1, 0, 1, 0), (1, 1, 1, 0), (1, 1, 1, 1), (1, 1, 0, 0), (0, 1, 1, 0)])
    )

    @pl.when(first == 1)
    def _():
        run_tiles(diag_work([(0, 0, 1, 0), (0, 1, 1, 1)]))

    @pl.when(first == 0)
    def _():
        run_tiles(diag_work([(1, 0, 0, 0), (1, 1, 0, 1)]))

    @pl.when((level > 1) & (is_top * odd == 1))
    def _():
        relay(2, second)

    phase("far_loop")

    @pl.loop(1, job_level + 1)
    def _(j):
        absorb(j, second, (0, 1))

        @pl.when((j > 1) & (j < level) & relays)
        def _():
            relay(j + 1, second)

    phase("w_side")
    for c in range(W_PARTS):
        w_side(c).wait_recv()
        w_pass(1 - side, 1, c).start()

    phase("finalize")
    lam_copy.wait_recv()
    for h in range(per):
        inverse = 1.0 / total[h : h + 1]
        mapped = acc[h] * inverse
        factor = lamb[swapped, side * per + h][0:1, 0:1]
        attn = mapped[:, :queries] - factor * mapped[:, queries:]
        scale = lax.rsqrt(jnp.mean(attn * attn, axis=0, keepdims=True) + eps)
        result = ((attn * scale).T * sub_ref[...]).astype(jnp.bfloat16)
        for ph in range(2):
            for which in range(2):
                at = ph * rows + which * half
                obuf[q_rows(which, pairs[ph]), h * vsize : (h + 1) * vsize] = result[
                    at : at + half
                ]
        logs = top[h : h + 1] + jnp.log(total[h : h + 1])
        for m in range(2):
            ordered = []
            for which in range(2):
                at = m * queries + which * half
                early, late = logs[:, at : at + half], logs[:, at + rows : at + rows + half]
                ordered.append(
                    jnp.concatenate(
                        [
                            jnp.where(first == 0, early, late),
                            jnp.where(first == 0, late, early),
                        ],
                        axis=1,
                    )
                )
            low, high = ordered
            lout[0, h, m : m + 1, :] = jnp.where(side == 0, low, high)
            lout[1, h, m : m + 1, :] = jnp.where(side == 0, high, low)

    phase("send_o")
    me8 = job_tp * 2 + side

    def piece_rows(which, target):
        return pl.ds(pl.multiple_of(which * rows + target * own, own), own)

    def o_copy(which, target, index):
        return remote(
            obuf.at[piece_rows(which, target)], hin.at[me8], o_send.at[index], o_recv.at[me8],
            {"sp": job_level * 2 + which, "tp": target},
        )

    def o_wait(which, source, index):
        spot = hin.at[source * 2 + which]
        return remote(spot, spot, o_send.at[index], o_recv.at[source * 2 + which], mate_id)

    peers = [(1 - side, diag), (1 - side, away), (side, diag), (side, away)]
    peers += [(1 - side, t), (1 - side, near), (side, near)]
    for index, (which, target) in enumerate(peers):
        o_copy(which, target, index).start()
    def log_copy(index):
        which = side + index - 2 * index * side
        return remote(
            lout.at[index], lin.at[index], log_send.at[index], log_recv.at[index],
            {"sp": job_level * 2 + which, "tp": job_tp},
        )

    log_copy(1).start()

    @pl.when(swaps)
    def _():
        o_copy(side, t, 7).start()
        log_copy(0).start()

    @pl.when(jnp.logical_not(swaps))
    def _():
        hin[me8] = obuf[piece_rows(side, t)]
        for h in range(per):
            log_ref[side * per + h] = lout[0, h]

    phase("conv_sum")
    fin_copy.wait_recv()
    far_sum.wait_recv()
    out_ref[...] += fin_in[...].astype(jnp.float32) + far_in[...].astype(jnp.float32)
    phase("w_wait")
    load_wa.wait()
    w_near.wait_recv()
    for c in range(W_PARTS):
        w_pass(side, 0, c).wait_recv()
        w_pass(1 - side, 1, c).wait_recv()
    phase("o_wait")
    for index, (which, source) in enumerate(peers):
        o_wait(which, source, index).wait_recv()

    @pl.when(swaps)
    def _():
        o_wait(side, t, 7).wait_recv()
        log_copy(0).wait_recv()
        for h in range(per):
            log_ref[side * per + h] = lin[0, h]

    phase("last_dot")
    lhs = jnp.concatenate([hin[i] for i in range(2 * tp)], axis=1)
    out_ref[...] += jnp.dot(lhs, wfull[...], preferred_element_type=jnp.float32)
    phase("log")
    log_copy(1).wait_recv()
    for h in range(per):
        log_ref[(1 - side) * per + h] = lin[1, h]

    phase("sends")
    near_copy.wait_send()
    for copy in far_copies + forwards:
        copy.wait_send()
    for pair in range(2):
        give_copy(pair).wait_send()
        giveq_copy(pair).wait_send()
    w_near.wait_send()
    for c in range(W_PARTS):
        for copy in (w_far(c), w_side(c), w_pass(side, 0, c), w_pass(1 - side, 1, c)):
            copy.wait_send()
    for copy in (cross_copy, fin_copy, far_sum, log_copy(1), lam_copy):
        copy.wait_send()
    for index, (which, target) in enumerate(peers):
        o_copy(which, target, index).wait_send()

    @pl.when(swaps)
    def _():
        o_copy(side, t, 7).wait_send()
        log_copy(0).wait_send()
        for which in range(2):
            for pair in range(2):
                swap_q(which, pair).wait_send()

    @pl.loop(is_top * (1 - odd) * level, level + 1 - is_top * odd)
    def _(lev):
        for pair in range(2):
            for which in range(2):
                up_copy(lev, pair, which).wait_send()

    @pl.when(s < sp - 1)
    def _():
        tail_copy.wait_send()

    phase(None)


def phase(name):
    pass


def vmem():
    return pl.BlockSpec(memory_space=pltpu.VMEM)


def on_device(
    inputs, norm_gain, w_query, w_key, w_value, query_gain, key_gain, lambdas, sub_gain,
    w_gate_b, w_gate_c, w_conv_in, conv_taps, conv_gain, w_out_att, w_out_conv,
):
    heads = lambdas.shape[0]
    comp = query_gain.shape[1]
    vsize = sub_gain.shape[0]
    channels = conv_gain.shape[0]
    own, width = inputs.shape
    tp = lax.axis_size("tp")
    sp = lax.axis_size("sp")
    rows = own * tp
    half = rows // 2
    qcols = heads * 2 * comp
    mine = qcols // 2
    per = heads // 2
    dma = pltpu.SemaphoreType.DMA
    bf, f32 = jnp.bfloat16, jnp.float32
    weights = (w_key, w_value, w_query, w_gate_c, w_conv_in, w_gate_b, w_out_att, w_out_conv)
    groups = sp // 2 * 4
    piece = pltpu.VMEM((own, width), bf)
    any_spec = pl.BlockSpec(memory_space=pl.ANY)
    mixed, log_sums = pl.pallas_call(
        functools.partial(layer, sp, tp, comp, heads),
        out_shape=(
            jax.ShapeDtypeStruct((own, width), f32),
            jax.ShapeDtypeStruct((heads, 2, rows), f32),
        ),
        in_specs=[vmem()] * 4 + [pl.BlockSpec(memory_space=pltpu.SMEM)] + [vmem()] * 3
        + [any_spec] * 8,
        out_specs=(vmem(), vmem()),
        scratch_shapes=[
            pltpu.VMEM((rows, width), bf),
            pltpu.VMEM((6, width, qcols), bf),
            pltpu.VMEM((tp * w_out_att.shape[0], width), bf),
            pltpu.VMEM(w_out_conv.shape, bf),
            pltpu.VMEM((8, qcols), f32),
            pltpu.VMEM((2, sp, 2 * half, 2 * mine), bf),
            pltpu.VMEM((3, per, vsize, 2 * half), bf),
            pltpu.VMEM((2, 2 * rows, mine), bf),
            pltpu.VMEM((2, half, 2 * mine), bf),
            pltpu.VMEM((2, half, mine), bf),
            pltpu.VMEM((per, 4 * rows, 2 * comp), bf),
            pltpu.VMEM((per, 4 * rows), f32),
            pltpu.VMEM((per, 4 * rows), f32),
            pltpu.VMEM((per, vsize, 4 * rows), f32),
            pltpu.VMEM((rows, 3 * channels), bf),
            pltpu.VMEM((EDGE, 2 * channels), bf),
            pltpu.VMEM((EDGE + rows, channels), f32),
            pltpu.VMEM((rows, channels), bf),
            pltpu.VMEM((2, heads, 8, 128), f32),
            piece, piece, piece, piece, piece, piece,
            pltpu.VMEM((2 * rows, per * vsize), bf),
            pltpu.VMEM((2 * tp, own, per * vsize), bf),
            pltpu.VMEM((2, per, 2, rows), f32),
            pltpu.VMEM((2, per, 2, rows), f32),
            dma((8,)), dma((2,)), dma((CHUNKS,)), dma((CHUNKS,)), dma((CHUNKS,)), dma((CHUNKS,)),
            dma((groups,)), dma((2 * groups,)), dma((2,)), dma((2,)), dma((2,)), dma((2,)),
            dma((9,)), dma((9,)), dma(()), dma(()), dma(()), dma(()), dma(()), dma(()),
            dma((8,)), dma((2 * tp,)), dma((2,)), dma((2,)), dma((2,)), dma((4,)), dma((4,)),
        ],
        compiler_params=pltpu.CompilerParams(
            collective_id=0, has_side_effects=True, vmem_limit_bytes=VMEM_LIMIT
        ),
        name="layer",
    )(
        inputs, norm_gain[None], query_gain, key_gain, lambdas, sub_gain[None], conv_taps,
        conv_gain[None], *weights,
    )
    return (mixed, log_sums)


def solution(mesh):
    in_specs = (
        P(("sp", "tp"), None),
        P(),
        P(None, "tp"),
        P(None, "tp"),
        P(None, "tp"),
        P(),
        P(),
        P("tp"),
        P(),
        P(None, "tp"),
        P(None, "tp"),
        P(None, "tp"),
        P(None, "tp"),
        P("tp"),
        P("tp", None),
        P("tp", None),
    )
    out_specs = (P(("sp", "tp"), None), P("tp", None, "sp"))
    return jax.shard_map(
        on_device, mesh=mesh, in_specs=in_specs, out_specs=out_specs, check_vma=False
    )
```

time: 57.8 us -> 54.5 us (0.943)
  the two profiles are of different devices: /device:TPU:25 before, /device:TPU:17 now
where the time goes in v3:
time: 54.5 us; the launch traced here: 54.4 us
  Pallas kernels  50.8 us (93%)
  local copies, waits for them, and re-layouts  2.9 us (5%)
  between operations  0.65 us (1%)
    pallas_call x1, Pallas kernels, on_device(): pl.pallas_call(functools.partial(layer, sp, tp, comp, heads), out_shape=(...  50.8 us
    unnamed x4, local copies, waits for them, and re-layouts  2.9 us

profile of v3, /device:TPU:17, one launch (start us, length us, event | category | flops | bytes accessed | tf_op | source)
XLA Modules:
  0.0 54.4 jit_solution(8383394038310587368)
XLA Ops:
  0.6 50.8 %layer.1 = (f32[128,2048]{1,0:T(8,128)}, f32[2,2,512]{2,1,0:T(2,128)}) custom-call(bf16[128,2048]{1,0:T(8,128)(2,1)} %x_ref.1, f32[1,2048]{1,0:T(1,128)} %bitcast.3, f32[2,64]{1,0:T(2,128)} %qg_ref.1, f32[2,64]{1,0:T(2,128)} %kg_ref.1, f32[2]{0:T(128)} %lam_ref.1, f32[1,128]{1,0:T(1,128)} %bitcast.5, f32[3,256]{1,0:T(4,128)} %taps_ref.1, f32[1,256]{1,0:T(1,128)} %bitcast.4, ...), custom_call_target="tpu_custom_call" | custom-call | tf_op jit(solution)/shard_map/layer/pallas_call | solution.py:822
  51.5 0.0 copy-start
  51.5 2.3 %copy.20 = f32[128,2048]{1,0:T(8,128)} copy(f32[128,2048]{1,0:T(8,128)} %get-tuple-element.4) | data formatting | bytes 2097152
  53.8 0.0 copy-done
  53.8 0.6 %copy.21 = f32[2,2,512]{2,1,0:T(2,128)} copy(f32[2,2,512]{2,1,0:T(2,128)S(1)} %copy-done) | data formatting | bytes 16384
Async XLA Ops:
  51.5 2.3 %copy-start = (f32[2,2,512]{2,1,0:T(2,128)S(1)}, f32[2,2,512]{2,1,0:T(2,128)}, u32[]{:S(2)}) copy-start(f32[2,2,512]{2,1,0:T(2,128)} %get-tuple-element.5) | copy-start | bytes 24580

commit v4 on v3

--- a/solution.py
+++ b/solution.py
@@ -51,12 +51,12 @@
     sp, tp, comp, heads,
     x_ref, gain_ref, qg_ref, kg_ref, lam_ref, sub_ref, taps_ref, cgain_ref,
     wk, wv, wq, wc, wi, wb, wa, wo,
-    out_ref, log_ref,
+    out_hbm, log_hbm, out_ref, log_ref,
     held, wbuf, wfull, wobuf, gains, kvb, vt, qb, give_kv, give_q, qpad, top, total, acc, cbuf, tail,
     padded, cvout, lamb, cross, fin, far, cross_in, fin_in, far_in, obuf, hin, lout, lin,
     wsem, near_sem, far_send, far_recv, fwd_send, fwd_recv, up_send, kv_recv, gk_send, gq_send,
-    q_recv, tail_sem, w_send, w_recv, cross_send, cross_recv, fin_send, fin_recv, fs_send, fs_recv,
-    o_send, o_recv, log_send, log_recv, lam_sem, qs_send, qs_recv,
+    q_recv, x_recv, tail_sem, w_send, w_recv, cross_send, cross_recv, fin_send, fin_recv, fs_send, fs_recv,
+    out_sem, o_send, o_recv, log_send, log_recv, lam_sem, qs_send, qs_recv,
 ):
     s = lax.axis_index("sp")
     t = lax.axis_index("tp")
@@ -242,19 +242,31 @@
         g = group_of(lev, pair, which)
         remote(spot, spot, up_send.at[g], kv_recv.at[where * groups + g], up_id).wait_recv()
 
-    def give_copy(pair):
+    sub = own // 2
+
+    def part_span(base, part):
+        if part is None:
+            return pl.ds(pl.multiple_of(base, half), half)
+        return pl.ds(pl.multiple_of(base + part * own, own), own)
+
+    def give_copy(pair, part):
+        index = 0 if part is None else 1 + part
+        arrival = kv_recv.at[group_of(level, pair, side)] if part is None else x_recv.at[part]
         return remote(
-            give_kv.at[pair], kvb.at[0, slot_of(level, pair), side_rows(side)],
-            gk_send.at[pair], kv_recv.at[group_of(level, pair, side)], mate_id,
+            give_kv.at[pair, part_span(0, part)],
+            kvb.at[0, slot_of(level, pair), part_span(side * half, part)],
+            gk_send.at[index], arrival, mate_id,
         )
 
     def q_rows(which, pair):
         return pl.ds(pl.multiple_of(which * rows + pair * half, half), half)
 
-    def giveq_copy(pair):
+    def giveq_copy(pair, part):
+        index = 0 if part is None else 1 + part
         return remote(
-            give_q.at[pair], qb.at[0, q_rows(side, pair)], gq_send.at[pair], q_recv.at[pair],
-            mate_id,
+            give_q.at[pair, part_span(0, part)],
+            qb.at[0, part_span(side * rows + pair * half, part)],
+            gq_send.at[index], q_recv.at[index], mate_id,
         )
 
     def swap_q(which, pair):
@@ -283,8 +295,19 @@
             jnp.bfloat16
         )
 
-    def project_kv(pair):
-        block = held[pair_rows(pair)]
+    def source(pair, part):
+        if part is None:
+            return held[pair_rows(pair)]
+        return jnp.concatenate(
+            [
+                held[pl.ds(pl.multiple_of(pair * half + b * own + part * sub, sub), sub)]
+                for b in range(2)
+            ],
+            axis=0,
+        )
+
+    def project_kv(pair, part=None):
+        block = source(pair, part)
         slot = slot_of(level, pair)
         for i in range(2):
             if i == 0:
@@ -295,39 +318,51 @@
                 )
             keep, give = split(res)
             cols = slice(i * head_cols, (i + 1) * head_cols)
-            kvb[0, slot, side_rows(side), cols] = keep
-            give_kv[pair, :, cols] = give
-
-        give_copy(pair).start()
-
-        @pl.when(sends_own)
-        def _():
-            up_copy(level, pair, side).start()
-
-    def project_q(pair):
-        block = held[pair_rows(pair)]
+            kvb[0, slot, part_span(side * half, part), cols] = keep
+            give_kv[pair, part_span(0, part), cols] = give
+
+        give_copy(pair, part).start()
+        if part != 0:
+            @pl.when(sends_own)
+            def _():
+                up_copy(level, pair, side).start()
+
+    def project_q(pair, part=None):
+        block = source(pair, part)
         keep, give = split(scaled(block, 2, 1, comp ** (-0.5)))
-        qb[0, q_rows(side, pair)] = keep
-        give_q[pair] = give
-        giveq_copy(pair).start()
-        pass_q(side, pair)
-
-    def project_conv(pair):
-        block = held[pair_rows(pair)]
+        qb[0, part_span(side * rows + pair * half, part)] = keep
+        give_q[pair, part_span(0, part)] = give
+        giveq_copy(pair, part).start()
+        if part != 0:
+            pass_q(side, pair)
+
+    def project_conv(pair, part=None):
+        block = source(pair, part)
         for i in range(3):
-            cbuf[pair_rows(pair), i * channels : (i + 1) * channels] = jnp.dot(
-                block, wbuf[3 + i], preferred_element_type=jnp.float32
-            ).astype(jnp.bfloat16)
-
-    def await_mate(pair):
-        arrived(0, level, pair, 1 - side)
+            res = jnp.dot(block, wbuf[3 + i], preferred_element_type=jnp.float32).astype(
+                jnp.bfloat16
+            )
+            cols = slice(i * channels, (i + 1) * channels)
+            if part is None:
+                cbuf[pair_rows(pair), cols] = res
+            else:
+                for b in range(2):
+                    begin = pl.multiple_of(pair * half + b * own + part * sub, sub)
+                    cbuf[pl.ds(begin, sub), cols] = res[b * sub : (b + 1) * sub]
+
+    def await_mate(pair, parts):
+        if parts is None:
+            arrived(0, level, pair, 1 - side)
+        else:
+            for part in parts:
+                give_copy(pair, part).wait_recv()
 
         @pl.when(sends_own)
         def _():
             up_copy(level, pair, 1 - side).start()
 
-    def relay(j, pair):
-        for which in (side, 1 - side):
+    def relay(j, pair, sides=(side, 1 - side)):
+        for which in sides:
             arrived(0, level - j, pair, which)
             up_copy(level - j, pair, which).start()
 
@@ -347,6 +382,10 @@
                 at = phase_index * rows + which * half
                 qpad[h, at : at + half] = jnp.where(lane < comp, q, zero)
                 qpad[h, queries + at : queries + at + half] = jnp.where(lane < comp, zero, q)
+
+    def position(index):
+        low = index % own
+        return low // sub * own + index // own * sub + low % sub
 
     def run_tiles(work):
         def score(item):
@@ -369,7 +408,9 @@
                 ahead.append(score(work[index + DEPTH]))
             if mask is not None:
                 kpos = lax.broadcasted_iota(jnp.int32, scores.shape, 0)
-                qpos = mask + lax.broadcasted_iota(jnp.int32, scores.shape, 1)
+                qpos = mask[0] + lax.broadcasted_iota(jnp.int32, scores.shape, 1)
+                if mask[1]:
+                    kpos, qpos = position(kpos), position(qpos)
                 scores = jnp.where(kpos <= qpos, scores, -1e30)
             old = top[h : h + 1, at]
             new = jnp.maximum(old, jnp.max(scores, axis=0, keepdims=True))
@@ -401,9 +442,9 @@
             for which in range(2):
                 arrived(1, lev, pair, which)
 
-    def absorb(j, pair, phases):
+    def absorb(j, pair, phases, take):
         lev = job_level - j
-        if 0 in phases:
+        if take:
             taken(lev, pair)
         slot = slot_of(lev, pair)
         turn_values(slot, 0)
@@ -434,13 +475,13 @@
                 for m in range(2):
                     base = m * queries + q_ph * rows + q_side * half
                     for offset in range(0, half, tile):
-                        size = offset + tile if same else half
+                        size = offset + tile if same and q_ph == 0 else half
                         work.append(
                             (
                                 h, key_part(slot, h, k_side * half, size),
                                 value_part(1 + k_ph, h, k_side * half, size),
                                 slice(base + offset, base + offset + tile),
-                                offset if same else None,
+                                (offset, q_ph == 1) if same else None,
                             )
                         )
         return work
@@ -474,14 +515,23 @@
         tail_copy.start()
 
     phase("mate_first")
-    await_mate(first)
+    await_mate(first, None)
+    phase("part_a")
+    for c in range(CHUNKS // 2):
+        far_copies[c].wait_recv()
+        forwards[c].start()
+    for c in range(CHUNKS // 2):
+        forwards[c].wait_recv()
+    project_kv(second, 0)
+    project_q(second, 0)
+    project_conv(second, 0)
 
     phase("below_first")
     @pl.when(has_down & relays)
     def _():
         relay(1, first)
 
-    giveq_copy(first).wait_recv()
+    giveq_copy(first, None).wait_recv()
     pass_q(1 - side, first)
     phase("early")
     top[...] = jnp.full_like(top, -1e30)
@@ -493,9 +543,12 @@
         diag_ready(0)
         run_tiles(diag_work([(0, 0, 0, 0), (0, 1, 0, 0), (0, 1, 0, 1)]))
 
-    for c in range(CHUNKS - 1):
+    for c in range(CHUNKS // 2, CHUNKS - 1):
         far_copies[c].wait_recv()
         forwards[c].start()
+
+    for c in range(W_PARTS):
+        w_far(c).start()
 
     @pl.when(jnp.logical_not(swaps))
     def _():
@@ -504,45 +557,65 @@
     phase("far_wait")
     far_copies[CHUNKS - 1].wait_recv()
     forwards[CHUNKS - 1].start()
-    for c in range(W_PARTS):
-        w_far(c).start()
-    for copy in forwards:
+    for copy in forwards[CHUNKS // 2 :]:
         copy.wait_recv()
     phase("kv_second")
-    project_kv(second)
+    project_kv(second, 1)
     phase("q_second")
-    project_q(second)
+    project_q(second, 1)
+    phase("conv_second")
+    project_conv(second, 1)
+
+    @pl.when((s < sp - 1) & (first == 0))
+    def _():
+        tail_copy.start()
+
     phase("below_first2")
 
     @pl.when((level > 1) & relays)
     def _():
         relay(2, first)
 
-    phase("conv_second")
-    project_conv(second)
-
-    @pl.when((s < sp - 1) & (first == 0))
-    def _():
-        tail_copy.start()
+    phase("early2a")
+
+    @pl.when(swaps & relays)
+    def _():
+        early()
+
+    @pl.when(jnp.logical_not(swaps) & (job_level > 0))
+    def _():
+        absorb(1, first, (0,), True)
+
+    phase("mate_second")
+    await_mate(second, (0, 1))
+
+    @pl.when(swaps)
+    def _():
+        for part in range(2):
+            giveq_copy(second, part).wait_recv()
+        swap_q(1 - side, second).start()
 
     phase("early2")
 
-    @pl.when(swaps)
+    @pl.when(jnp.logical_not(relays))
     def _():
         early()
 
     @pl.when(relays)
     def _():
-        @pl.loop(1, jnp.minimum(job_level, 2) + 1)
+        @pl.loop(2 - swapped, jnp.minimum(job_level, 2) + 1)
         def _(j):
-            absorb(j, first, (0,))
-
-    phase("mate_second")
-    await_mate(second)
-
-    phase("qpad")
-    giveq_copy(second).wait_recv()
-    pass_q(1 - side, second)
+            absorb(j, first, (0,), True)
+
+    @pl.when(jnp.logical_not(swaps))
+    def _():
+        for part in range(2):
+            giveq_copy(second, part).wait_recv()
+
+    @pl.when(has_down & relays)
+    def _():
+        relay(1, second, (side,))
+
     phase("w_first")
     w_spread(0)
     phase("conv")
@@ -585,36 +658,65 @@
     out_ref[...] = partial(t)
     phase("relay_second")
 
-    @pl.when(has_down & relays)
-    def _():
-        relay(1, second)
+    @pl.when(has_down & (is_top == 0))
+    def _():
+        relay(1, second, (1 - side,))
+
+    def settle():
+        toward = partial(away)
+        cross_copy.wait_recv()
+        far[...] = (toward + cross_in[...].astype(jnp.float32)).astype(jnp.bfloat16)
+        far_sum.start()
+
+    @pl.when(jnp.logical_not(relays))
+    def _():
+        settle()
+
+    phase("q_late")
+    prepare(1, second)
+    phase("near1")
+
+    @pl.when(job_level > 0)
+    def _():
+        @pl.when(jnp.logical_not(relays))
+        def _():
+            absorb(1, first, (0,), True)
+
+        absorb(1, first, (1,), False)
 
     phase("toward")
-    toward = partial(away)
-    cross_copy.wait_recv()
-    far[...] = (toward + cross_in[...].astype(jnp.float32)).astype(jnp.bfloat16)
-    far_sum.start()
+
+    @pl.when(relays)
+    def _():
+        settle()
+
     phase("w_far")
     w_spread(1)
-    phase("q_late")
-    prepare(1, second)
+    @pl.when(has_down & (is_top * odd == 1))
+    def _():
+        relay(1, second, (1 - side,))
+
+    @pl.when((level > 1) & relays)
+    def _():
+        relay(2, second, (side,))
+
     phase("near_loop")
 
-    @pl.loop(1, job_level + 1)
+    @pl.loop(2, job_level + 1)
     def _(j):
-        @pl.when((j > 1) & (j < level) & relays)
+        @pl.when((j < level) & relays)
         def _():
             relay(j + 1, first)
 
-        @pl.when((j == job_level) & (level > 1) & (is_top == 0))
-        def _():
-            relay(2, second)
-
         @pl.when((j > 2) | jnp.logical_not(relays))
         def _():
-            absorb(j, first, (0,))
-
-        absorb(j, first, (1,))
+            absorb(j, first, (0,), True)
+
+        absorb(j, first, (1,), False)
+
+    @pl.when((level > 1) & relays)
+    def _():
+        relay(2, second, (1 - side,))
 
     phase("diag")
     diag_ready(1)
@@ -630,60 +732,6 @@
     def _():
         run_tiles(diag_work([(1, 0, 0, 0), (1, 1, 0, 1)]))
 
-    @pl.when((level > 1) & (is_top * odd == 1))
-    def _():
-        relay(2, second)
-
-    phase("far_loop")
-
-    @pl.loop(1, job_level + 1)
-    def _(j):
-        absorb(j, second, (0, 1))
-
-        @pl.when((j > 1) & (j < level) & relays)
-        def _():
-            relay(j + 1, second)
-
-    phase("w_side")
-    for c in range(W_PARTS):
-        w_side(c).wait_recv()
-        w_pass(1 - side, 1, c).start()
-
-    phase("finalize")
-    lam_copy.wait_recv()
-    for h in range(per):
-        inverse = 1.0 / total[h : h + 1]
-        mapped = acc[h] * inverse
-        factor = lamb[swapped, side * per + h][0:1, 0:1]
-        attn = mapped[:, :queries] - factor * mapped[:, queries:]
-        scale = lax.rsqrt(jnp.mean(attn * attn, axis=0, keepdims=True) + eps)
-        result = ((attn * scale).T * sub_ref[...]).astype(jnp.bfloat16)
-        for ph in range(2):
-            for which in range(2):
-                at = ph * rows + which * half
-                obuf[q_rows(which, pairs[ph]), h * vsize : (h + 1) * vsize] = result[
-                    at : at + half
-                ]
-        logs = top[h : h + 1] + jnp.log(total[h : h + 1])
-        for m in range(2):
-            ordered = []
-            for which in range(2):
-                at = m * queries + which * half
-                early, late = logs[:, at : at + half], logs[:, at + rows : at + rows + half]
-                ordered.append(
-                    jnp.concatenate(
-                        [
-                            jnp.where(first == 0, early, late),
-                            jnp.where(first == 0, late, early),
-                        ],
-                        axis=1,
-                    )
-                )
-            low, high = ordered
-            lout[0, h, m : m + 1, :] = jnp.where(side == 0, low, high)
-            lout[1, h, m : m + 1, :] = jnp.where(side == 0, high, low)
-
-    phase("send_o")
     me8 = job_tp * 2 + side
 
     def piece_rows(which, target):
@@ -695,14 +743,92 @@
             {"sp": job_level * 2 + which, "tp": target},
         )
 
-    def o_wait(which, source, index):
-        spot = hin.at[source * 2 + which]
-        return remote(spot, spot, o_send.at[index], o_recv.at[source * 2 + which], mate_id)
+    def o_wait(which, source_tp, index):
+        spot = hin.at[source_tp * 2 + which]
+        return remote(spot, spot, o_send.at[index], o_recv.at[source_tp * 2 + which], mate_id)
 
     peers = [(1 - side, diag), (1 - side, away), (side, diag), (side, away)]
     peers += [(1 - side, t), (1 - side, near), (side, near)]
-    for index, (which, target) in enumerate(peers):
+
+    def conclude(ph):
+        span = slice(ph * rows, (ph + 1) * rows)
+        other = slice(queries + ph * rows, queries + (ph + 1) * rows)
+        for h in range(per):
+            factor = lamb[swapped, side * per + h][0:1, 0:1]
+            attn = acc[h, :, span] * (1.0 / total[h : h + 1, span])
+            attn = attn - factor * (acc[h, :, other] * (1.0 / total[h : h + 1, other]))
+            scale = lax.rsqrt(jnp.mean(attn * attn, axis=0, keepdims=True) + eps)
+            result = ((attn * scale).T * sub_ref[...]).astype(jnp.bfloat16)
+            cols = slice(h * vsize, (h + 1) * vsize)
+            for which in range(2):
+                base = which * half
+                if ph == 0:
+                    obuf[q_rows(which, first), cols] = result[base : base + half]
+                else:
+                    for part in range(2):
+                        for b in range(2):
+                            begin = which * rows + second * half + b * own + part * sub
+                            at = base + part * own + b * sub
+                            obuf[pl.ds(pl.multiple_of(begin, sub), sub), cols] = result[
+                                at : at + sub
+                            ]
+
+    def store_logs():
+        for h in range(per):
+            logs = top[h : h + 1] + jnp.log(total[h : h + 1])
+            for m in range(2):
+                ordered = []
+                for which in range(2):
+                    at = m * queries + which * half
+                    early_part = logs[:, at : at + half]
+                    late_part = jnp.concatenate(
+                        [
+                            logs[:, at + rows + part * own + b * sub :][:, :sub]
+                            for b in range(2)
+                            for part in range(2)
+                        ],
+                        axis=1,
+                    )
+                    ordered.append(
+                        jnp.concatenate(
+                            [
+                                jnp.where(first == 0, early_part, late_part),
+                                jnp.where(first == 0, late_part, early_part),
+                            ],
+                            axis=1,
+                        )
+                    )
+                low, high = ordered
+                lout[0, h, m : m + 1, :] = jnp.where(side == 0, low, high)
+                lout[1, h, m : m + 1, :] = jnp.where(side == 0, high, low)
+
+    phase("far_loop")
+
+    @pl.loop(1, job_level + 1)
+    def _(j):
+        absorb(j, second, (1,), True)
+
+        @pl.when((j > 1) & (j < level) & relays)
+        def _():
+            relay(j + 1, second)
+
+    phase("finish1")
+    lam_copy.wait_recv()
+    conclude(1)
+    for index in range(4):
+        which, target = peers[index]
         o_copy(which, target, index).start()
+    phase("far_loop0")
+
+    @pl.loop(1, job_level + 1)
+    def _(j):
+        absorb(j, second, (0,), False)
+
+    phase("w_side")
+    for c in range(W_PARTS):
+        w_side(c).wait_recv()
+        w_pass(1 - side, 1, c).start()
+
     def log_copy(index):
         which = side + index - 2 * index * side
         return remote(
@@ -710,11 +836,21 @@
             {"sp": job_level * 2 + which, "tp": job_tp},
         )
 
+    phase("finish0")
+    conclude(0)
+    for index in range(4, 7):
+        which, target = peers[index]
+        o_copy(which, target, index).start()
+
+    @pl.when(swaps)
+    def _():
+        o_copy(side, t, 7).start()
+
+    store_logs()
     log_copy(1).start()
 
     @pl.when(swaps)
     def _():
-        o_copy(side, t, 7).start()
         log_copy(0).start()
 
     @pl.when(jnp.logical_not(swaps))
@@ -744,21 +880,32 @@
         for h in range(per):
             log_ref[side * per + h] = lin[0, h]
 
-    phase("last_dot")
-    lhs = jnp.concatenate([hin[i] for i in range(2 * tp)], axis=1)
-    out_ref[...] += jnp.dot(lhs, wfull[...], preferred_element_type=jnp.float32)
     phase("log")
     log_copy(1).wait_recv()
     for h in range(per):
         log_ref[(1 - side) * per + h] = lin[1, h]
-
+    log_store = pltpu.make_async_copy(log_ref, log_hbm, out_sem.at[CHUNKS])
+    log_store.start()
+
+    phase("last_dot")
+    lhs = jnp.concatenate([hin[i] for i in range(2 * tp)], axis=1)
+    strip = out_ref.shape[1] // CHUNKS
+    stores = [log_store]
+    for c in range(CHUNKS):
+        cols = slice(c * strip, (c + 1) * strip)
+        out_ref[:, cols] += jnp.dot(lhs, wfull[:, cols], preferred_element_type=jnp.float32)
+        store = pltpu.make_async_copy(out_ref.at[:, cols], out_hbm.at[:, cols], out_sem.at[c])
+        store.start()
+        stores.append(store)
     phase("sends")
+    for store in stores:
+        store.wait()
     near_copy.wait_send()
     for copy in far_copies + forwards:
         copy.wait_send()
-    for pair in range(2):
-        give_copy(pair).wait_send()
-        giveq_copy(pair).wait_send()
+    for pair, part in ((first, None), (second, 0), (second, 1)):
+        give_copy(pair, part).wait_send()
+        giveq_copy(pair, part).wait_send()
     w_near.wait_send()
     for c in range(W_PARTS):
         for copy in (w_far(c), w_side(c), w_pass(side, 0, c), w_pass(1 - side, 1, c)):
@@ -827,8 +974,10 @@
         ),
         in_specs=[vmem()] * 4 + [pl.BlockSpec(memory_space=pltpu.SMEM)] + [vmem()] * 3
         + [any_spec] * 8,
-        out_specs=(vmem(), vmem()),
+        out_specs=(any_spec, any_spec),
         scratch_shapes=[
+            pltpu.VMEM((own, width), f32),
+            pltpu.VMEM((heads, 2, rows), f32),
             pltpu.VMEM((rows, width), bf),
             pltpu.VMEM((6, width, qcols), bf),
             pltpu.VMEM((tp * w_out_att.shape[0], width), bf),
@@ -854,9 +1003,11 @@
             pltpu.VMEM((2, per, 2, rows), f32),
             pltpu.VMEM((2, per, 2, rows), f32),
             dma((8,)), dma((2,)), dma((CHUNKS,)), dma((CHUNKS,)), dma((CHUNKS,)), dma((CHUNKS,)),
-            dma((groups,)), dma((2 * groups,)), dma((2,)), dma((2,)), dma((2,)), dma((2,)),
+            dma((groups,)), dma((2 * groups,)), dma((3,)), dma((3,)), dma((3,)), dma((2,)),
+            dma((2,)),
             dma((9,)), dma((9,)), dma(()), dma(()), dma(()), dma(()), dma(()), dma(()),
-            dma((8,)), dma((2 * tp,)), dma((2,)), dma((2,)), dma((2,)), dma((4,)), dma((4,)),
+            dma((CHUNKS + 1,)), dma((8,)), dma((2 * tp,)), dma((2,)), dma((2,)), dma((2,)),
+            dma((4,)), dma((4,)),
         ],
         compiler_params=pltpu.CompilerParams(
             collective_id=0, has_side_effects=True, vmem_limit_bytes=VMEM_LIMIT

time: 54.5 us -> 53 us (0.972)
  Pallas kernels: 50.8 us -> 49.3 us
    pallas_call x1, Pallas kernels: 50.8 us -> 49.3 us  [on_device(): pl.pallas_call(functools.partial(layer, sp, tp, comp, heads), out_shape=(...]
where the time goes in v4:
time: 53 us; the launch traced here: 52.8 us
  Pallas kernels  49.3 us (93%)
  local copies, waits for them, and re-layouts  2.9 us (5%)
  between operations  0.65 us (1%)
    pallas_call x1, Pallas kernels, on_device(): pl.pallas_call(functools.partial(layer, sp, tp, comp, heads), out_shape=(...  49.3 us
    unnamed x4, local copies, waits for them, and re-layouts  2.9 us

profile of v4, /device:TPU:17, one launch (start us, length us, event | category | flops | bytes accessed | tf_op | source)
XLA Modules:
  0.0 52.8 jit_solution(17409870940892088949)
XLA Ops:
  0.6 49.3 %layer.1 = (f32[128,2048]{1,0:T(8,128)}, f32[2,2,512]{2,1,0:T(2,128)}) custom-call(bf16[128,2048]{1,0:T(8,128)(2,1)} %x_ref.1, f32[1,2048]{1,0:T(1,128)} %bitcast.3, f32[2,64]{1,0:T(2,128)} %qg_ref.1, f32[2,64]{1,0:T(2,128)} %kg_ref.1, f32[2]{0:T(128)} %lam_ref.1, f32[1,128]{1,0:T(1,128)} %bitcast.5, f32[3,256]{1,0:T(4,128)} %taps_ref.1, f32[1,256]{1,0:T(1,128)} %bitcast.4, ...), custom_call_target="tpu_custom_call" | custom-call | tf_op jit(solution)/shard_map/layer/pallas_call | solution.py:969
  49.9 0.0 copy-start
  49.9 2.3 %copy.20 = f32[128,2048]{1,0:T(8,128)} copy(f32[128,2048]{1,0:T(8,128)} %get-tuple-element.4) | data formatting | bytes 2097152
  52.2 0.0 copy-done
  52.2 0.6 %copy.21 = f32[2,2,512]{2,1,0:T(2,128)} copy(f32[2,2,512]{2,1,0:T(2,128)S(1)} %copy-done) | data formatting | bytes 16384
Async XLA Ops:
  49.9 2.3 %copy-start = (f32[2,2,512]{2,1,0:T(2,128)S(1)}, f32[2,2,512]{2,1,0:T(2,128)}, u32[]{:S(2)}) copy-start(f32[2,2,512]{2,1,0:T(2,128)} %get-tuple-element.5) | copy-start | bytes 24580

commit v5 on v4

--- a/solution.py
+++ b/solution.py
@@ -49,9 +49,10 @@
 
 def layer(
     sp, tp, comp, heads,
-    x_ref, gain_ref, qg_ref, kg_ref, lam_ref, sub_ref, taps_ref, cgain_ref,
+    x_in, gain_in, qg_in, kg_in, lam_in, sub_in, taps_in, cgain_in,
     wk, wv, wq, wc, wi, wb, wa, wo,
-    out_hbm, log_hbm, out_ref, log_ref,
+    out_hbm, log_hbm, x_ref, gain_ref, qg_ref, kg_ref, lam_ref, sub_ref, taps_ref, cgain_ref,
+    in_sem, out_ref, log_ref,
     held, wbuf, wfull, wobuf, gains, kvb, vt, qb, give_kv, give_q, qpad, top, total, acc, cbuf, tail,
     padded, cvout, lamb, cross, fin, far, cross_in, fin_in, far_in, obuf, hin, lout, lin,
     wsem, near_sem, far_send, far_recv, fwd_send, fwd_recv, up_send, kv_recv, gk_send, gq_send,
@@ -99,12 +100,19 @@
     relays = is_top * (1 - odd) == 0
     groups = sp // 2 * 4
 
+    small = (
+        (x_in, x_ref), (gain_in, gain_ref), (kg_in, kg_ref), (qg_in, qg_ref), (lam_in, lam_ref),
+        (sub_in, sub_ref), (taps_in, taps_ref), (cgain_in, cgain_ref),
+    )
+    reads = [
+        pltpu.make_async_copy(src, dst, in_sem.at[i]) for i, (src, dst) in enumerate(small)
+    ]
+    for read in reads:
+        read.start()
     loads = [
         pltpu.make_async_copy(w, wbuf.at[i], wsem.at[i])
         for i, w in enumerate((wk, wv, wq, wc, wi, wb))
     ]
-    for load in loads:
-        load.start()
     wa_rows = wa.shape[0]
     half_rows = wa_rows // 2
 
@@ -119,13 +127,51 @@
 
     load_wa = pltpu.make_async_copy(wa, wfull.at[shard(t)], wsem.at[6])
     load_wo = pltpu.make_async_copy(wo, wobuf, wsem.at[7])
-    load_wa.start()
-    load_wo.start()
 
     def block_at(index):
         return pl.ds(pl.multiple_of(index * own, own), own)
 
+    phase("barrier")
+    barrier = pltpu.get_barrier_semaphore()
+
+    def hello(where):
+        pl.semaphore_signal(barrier, inc=1, device_id=where, device_id_type=MESH)
+
+    for peer in (near, away, diag):
+        hello({"tp": peer})
+    for peer in (t, near, away, diag):
+        hello({"sp": mate, "tp": peer})
+
+    plain_up = level < levels - 2
+    plain_down = has_down & (level < levels - 1)
+
+    @pl.when(plain_up)
+    def _():
+        hello({"sp": s + 2})
+
+    @pl.when(plain_down)
+    def _():
+        hello({"sp": s - 2})
+
+    @pl.when(high_pair == 1)
+    def _():
+        for which in range(2):
+            for peer in range(tp):
+                hello({"sp": (cross_sp // 2) * 2 + which, "tp": peer})
+
+    @pl.when((side == 1) & has_up)
+    def _():
+        hello({"sp": s + 1})
+
+    @pl.when((side == 0) & has_down)
+    def _():
+        hello({"sp": s - 1})
+
     phase("norm")
+    for read in reads:
+        read.wait()
+    for load in (*loads, load_wa, load_wo):
+        load.start()
     x = x_ref[...].astype(jnp.float32)
     held[block_at(t), :] = (rms_scale(x) * gain_ref[...]).astype(jnp.bfloat16)
     for row, ref in ((0, kg_ref), (1, qg_ref)):
@@ -134,42 +180,7 @@
                 at = (h * 2 + m) * comp
                 gains[row : row + 1, at : at + comp] = ref[m : m + 1, :]
 
-    phase("barrier")
-    barrier = pltpu.get_barrier_semaphore()
-
-    def hello(where):
-        pl.semaphore_signal(barrier, inc=1, device_id=where, device_id_type=MESH)
-
-    for peer in (near, away, diag):
-        hello({"tp": peer})
-    for peer in (t, near, away, diag):
-        hello({"sp": mate, "tp": peer})
-
-    plain_up = level < levels - 2
-    plain_down = has_down & (level < levels - 1)
-
-    @pl.when(plain_up)
-    def _():
-        hello({"sp": s + 2})
-
-    @pl.when(plain_down)
-    def _():
-        hello({"sp": s - 2})
-
-    @pl.when(high_pair == 1)
-    def _():
-        for which in range(2):
-            for peer in range(tp):
-                hello({"sp": (cross_sp // 2) * 2 + which, "tp": peer})
-
-    @pl.when((side == 1) & has_up)
-    def _():
-        hello({"sp": s + 1})
-
-    @pl.when((side == 0) & has_down)
-    def _():
-        hello({"sp": s - 1})
-
+    phase("barrier_wait")
     expected = 7 + as_int(plain_up) + as_int(plain_down) + 2 * tp * high_pair
     pl.semaphore_wait(barrier, expected + side * ups + (1 - side) * downs)
 
@@ -696,10 +707,6 @@
     def _():
         relay(1, second, (1 - side,))
 
-    @pl.when((level > 1) & relays)
-    def _():
-        relay(2, second, (side,))
-
     phase("near_loop")
 
     @pl.loop(2, job_level + 1)
@@ -713,6 +720,10 @@
             absorb(j, first, (0,), True)
 
         absorb(j, first, (1,), False)
+
+        @pl.when((j == 2) & (level > 1) & relays)
+        def _():
+            relay(2, second, (side,))
 
     @pl.when((level > 1) & relays)
     def _():
@@ -837,6 +848,13 @@
         )
 
     phase("finish0")
+    store_logs()
+    log_copy(1).start()
+
+    @pl.when(swaps)
+    def _():
+        log_copy(0).start()
+
     conclude(0)
     for index in range(4, 7):
         which, target = peers[index]
@@ -845,13 +863,6 @@
     @pl.when(swaps)
     def _():
         o_copy(side, t, 7).start()
-
-    store_logs()
-    log_copy(1).start()
-
-    @pl.when(swaps)
-    def _():
-        log_copy(0).start()
 
     @pl.when(jnp.logical_not(swaps))
     def _():
@@ -880,23 +891,23 @@
         for h in range(per):
             log_ref[side * per + h] = lin[0, h]
 
+    phase("last_dot")
+    lhs = jnp.concatenate([hin[i] for i in range(2 * tp)], axis=1)
+    strip = out_ref.shape[1] // CHUNKS
+    stores = []
+    for c in range(CHUNKS):
+        cols = slice(c * strip, (c + 1) * strip)
+        out_ref[:, cols] += jnp.dot(lhs, wfull[:, cols], preferred_element_type=jnp.float32)
+        store = pltpu.make_async_copy(out_ref.at[:, cols], out_hbm.at[:, cols], out_sem.at[c])
+        store.start()
+        stores.append(store)
     phase("log")
     log_copy(1).wait_recv()
     for h in range(per):
         log_ref[(1 - side) * per + h] = lin[1, h]
     log_store = pltpu.make_async_copy(log_ref, log_hbm, out_sem.at[CHUNKS])
     log_store.start()
-
-    phase("last_dot")
-    lhs = jnp.concatenate([hin[i] for i in range(2 * tp)], axis=1)
-    strip = out_ref.shape[1] // CHUNKS
-    stores = [log_store]
-    for c in range(CHUNKS):
-        cols = slice(c * strip, (c + 1) * strip)
-        out_ref[:, cols] += jnp.dot(lhs, wfull[:, cols], preferred_element_type=jnp.float32)
-        store = pltpu.make_async_copy(out_ref.at[:, cols], out_hbm.at[:, cols], out_sem.at[c])
-        store.start()
-        stores.append(store)
+    stores.append(log_store)
     phase("sends")
     for store in stores:
         store.wait()
@@ -938,10 +949,6 @@
 
 def phase(name):
     pass
-
-
-def vmem():
-    return pl.BlockSpec(memory_space=pltpu.VMEM)
 
 
 def on_device(
@@ -972,10 +979,18 @@
             jax.ShapeDtypeStruct((own, width), f32),
             jax.ShapeDtypeStruct((heads, 2, rows), f32),
         ),
-        in_specs=[vmem()] * 4 + [pl.BlockSpec(memory_space=pltpu.SMEM)] + [vmem()] * 3
-        + [any_spec] * 8,
+        in_specs=[any_spec] * 16,
         out_specs=(any_spec, any_spec),
         scratch_shapes=[
+            pltpu.VMEM(inputs.shape, inputs.dtype),
+            pltpu.VMEM((1, width), f32),
+            pltpu.VMEM(query_gain.shape, f32),
+            pltpu.VMEM(key_gain.shape, f32),
+            pltpu.SMEM(lambdas.shape, f32),
+            pltpu.VMEM((1, vsize), f32),
+            pltpu.VMEM(conv_taps.shape, f32),
+            pltpu.VMEM((1, channels), f32),
+            dma((8,)),
             pltpu.VMEM((own, width), f32),
             pltpu.VMEM((heads, 2, rows), f32),
             pltpu.VMEM((rows, width), bf),

time: 53 us -> 50.5 us (0.953)
  Pallas kernels: 49.3 us -> 46.8 us
    pallas_call x1, Pallas kernels: 49.3 us -> 46.8 us  [on_device(): pl.pallas_call(functools.partial(layer, sp, tp, comp, heads), out_shape=(...]
where the time goes in v5:
time: 50.5 us; the launch traced here: 50.4 us
  Pallas kernels  46.8 us (93%)
  local copies, waits for them, and re-layouts  2.9 us (6%)
  between operations  0.65 us (1%)
    pallas_call x1, Pallas kernels, on_device(): pl.pallas_call(functools.partial(layer, sp, tp, comp, heads), out_shape=(...  46.8 us
    unnamed x4, local copies, waits for them, and re-layouts  2.9 us

profile of v5, /device:TPU:17, one launch (start us, length us, event | category | flops | bytes accessed | tf_op | source)
XLA Modules:
  0.0 50.4 jit_solution(3233235734851883812)
XLA Ops:
  0.6 46.8 %layer.1 = (f32[128,2048]{1,0:T(8,128)}, f32[2,2,512]{2,1,0:T(2,128)}) custom-call(bf16[128,2048]{1,0:T(8,128)(2,1)} %x_in.1, f32[1,2048]{1,0:T(1,128)} %bitcast.3, f32[2,64]{1,0:T(2,128)} %qg_in.1, f32[2,64]{1,0:T(2,128)} %kg_in.1, f32[2]{0:T(128)} %lam_in.1, f32[1,128]{1,0:T(1,128)} %bitcast.5, f32[3,256]{1,0:T(4,128)} %taps_in.1, f32[1,256]{1,0:T(1,128)} %bitcast.4, ...), custom_call_target="tpu_custom_call" | custom-call | tf_op jit(solution)/shard_map/layer/pallas_call | solution.py:976
  47.5 0.0 copy-start
  47.5 2.3 %copy.20 = f32[128,2048]{1,0:T(8,128)} copy(f32[128,2048]{1,0:T(8,128)} %get-tuple-element.4) | data formatting | bytes 2097152
  49.8 0.0 copy-done
  49.8 0.6 %copy.21 = f32[2,2,512]{2,1,0:T(2,128)} copy(f32[2,2,512]{2,1,0:T(2,128)S(1)} %copy-done) | data formatting | bytes 16384
Async XLA Ops:
  47.5 2.3 %copy-start = (f32[2,2,512]{2,1,0:T(2,128)S(1)}, f32[2,2,512]{2,1,0:T(2,128)}, u32[]{:S(2)}) copy-start(f32[2,2,512]{2,1,0:T(2,128)} %get-tuple-element.5) | copy-start | bytes 24580

commit v6 on v5

--- a/solution.py
+++ b/solution.py
@@ -52,12 +52,12 @@
     x_in, gain_in, qg_in, kg_in, lam_in, sub_in, taps_in, cgain_in,
     wk, wv, wq, wc, wi, wb, wa, wo,
     out_hbm, log_hbm, x_ref, gain_ref, qg_ref, kg_ref, lam_ref, sub_ref, taps_ref, cgain_ref,
-    in_sem, out_ref, log_ref,
+    out_ref, log_ref,
     held, wbuf, wfull, wobuf, gains, kvb, vt, qb, give_kv, give_q, qpad, top, total, acc, cbuf, tail,
     padded, cvout, lamb, cross, fin, far, cross_in, fin_in, far_in, obuf, hin, lout, lin,
     wsem, near_sem, far_send, far_recv, fwd_send, fwd_recv, up_send, kv_recv, gk_send, gq_send,
     q_recv, x_recv, tail_sem, w_send, w_recv, cross_send, cross_recv, fin_send, fin_recv, fs_send, fs_recv,
-    out_sem, o_send, o_recv, log_send, log_recv, lam_sem, qs_send, qs_recv,
+    o_send, o_recv, log_send, log_recv, lam_sem, qs_send, qs_recv,
 ):
     s = lax.axis_index("sp")
     t = lax.axis_index("tp")
@@ -105,7 +105,7 @@
         (sub_in, sub_ref), (taps_in, taps_ref), (cgain_in, cgain_ref),
     )
     reads = [
-        pltpu.make_async_copy(src, dst, in_sem.at[i]) for i, (src, dst) in enumerate(small)
+        pltpu.make_async_copy(src, dst, wsem.at[i]) for i, (src, dst) in enumerate(small)
     ]
     for read in reads:
         read.start()
@@ -317,8 +317,7 @@
             axis=0,
         )
 
-    def project_kv(pair, part=None):
-        block = source(pair, part)
+    def place_kv(block, pair, part):
         slot = slot_of(level, pair)
         for i in range(2):
             if i == 0:
@@ -332,6 +331,11 @@
             kvb[0, slot, part_span(side * half, part), cols] = keep
             give_kv[pair, part_span(0, part), cols] = give
 
+    def project_kv(pair, part):
+        place_kv(source(pair, part), pair, part)
+        send_kv(pair, part)
+
+    def send_kv(pair, part):
         give_copy(pair, part).start()
         if part != 0:
             @pl.when(sends_own)
@@ -504,10 +508,12 @@
     phase("wait_kv_weights")
     loads[0].wait()
     loads[1].wait()
+    place_kv(held[block_at(t)], first, odd)
     phase("wait_near")
     near_copy.wait_recv()
     phase("kv_first")
-    project_kv(first)
+    place_kv(held[block_at(near)], first, 1 - odd)
+    send_kv(first, None)
     w_near.start()
     phase("q_first")
     loads[2].wait()
@@ -898,14 +904,14 @@
     for c in range(CHUNKS):
         cols = slice(c * strip, (c + 1) * strip)
         out_ref[:, cols] += jnp.dot(lhs, wfull[:, cols], preferred_element_type=jnp.float32)
-        store = pltpu.make_async_copy(out_ref.at[:, cols], out_hbm.at[:, cols], out_sem.at[c])
+        store = pltpu.make_async_copy(out_ref.at[:, cols], out_hbm.at[:, cols], wsem.at[c])
         store.start()
         stores.append(store)
     phase("log")
     log_copy(1).wait_recv()
     for h in range(per):
         log_ref[(1 - side) * per + h] = lin[1, h]
-    log_store = pltpu.make_async_copy(log_ref, log_hbm, out_sem.at[CHUNKS])
+    log_store = pltpu.make_async_copy(log_ref, log_hbm, wsem.at[CHUNKS])
     log_store.start()
     stores.append(log_store)
     phase("sends")
@@ -949,6 +955,23 @@
 
 def phase(name):
     pass
+
+
+def deliver(mixed_in, log_in, mixed_out, log_out, mixed_buf, log_buf, read_sem, write_sem):
+    strip = mixed_buf.shape[0] // CHUNKS
+    spans = [(mixed_in, mixed_buf, mixed_out, pl.ds(c * strip, strip)) for c in range(CHUNKS)]
+    spans.append((log_in, log_buf, log_out, pl.ds(0, log_buf.shape[0])))
+    reads, writes = [], []
+    for i, (src, buf, dst, at) in enumerate(spans):
+        reads.append(pltpu.make_async_copy(src.at[at], buf.at[at], read_sem.at[i]))
+        writes.append(pltpu.make_async_copy(buf.at[at], dst.at[at], write_sem.at[i]))
+    for read in reads:
+        read.start()
+    for read, write in zip(reads, writes):
+        read.wait()
+        write.start()
+    for write in writes:
+        write.wait()
 
 
 def on_device(
@@ -990,7 +1013,6 @@
             pltpu.VMEM((1, vsize), f32),
             pltpu.VMEM(conv_taps.shape, f32),
             pltpu.VMEM((1, channels), f32),
-            dma((8,)),
             pltpu.VMEM((own, width), f32),
             pltpu.VMEM((heads, 2, rows), f32),
             pltpu.VMEM((rows, width), bf),
@@ -1021,7 +1043,7 @@
             dma((groups,)), dma((2 * groups,)), dma((3,)), dma((3,)), dma((3,)), dma((2,)),
             dma((2,)),
             dma((9,)), dma((9,)), dma(()), dma(()), dma(()), dma(()), dma(()), dma(()),
-            dma((CHUNKS + 1,)), dma((8,)), dma((2 * tp,)), dma((2,)), dma((2,)), dma((2,)),
+            dma((8,)), dma((2 * tp,)), dma((2,)), dma((2,)), dma((2,)),
             dma((4,)), dma((4,)),
         ],
         compiler_params=pltpu.CompilerParams(
@@ -1032,7 +1054,23 @@
         inputs, norm_gain[None], query_gain, key_gain, lambdas, sub_gain[None], conv_taps,
         conv_gain[None], *weights,
     )
-    return (mixed, log_sums)
+    return pl.pallas_call(
+        deliver,
+        out_shape=(
+            jax.ShapeDtypeStruct(mixed.shape, f32),
+            jax.ShapeDtypeStruct(log_sums.shape, f32),
+        ),
+        in_specs=[any_spec, any_spec],
+        out_specs=(any_spec, any_spec),
+        scratch_shapes=[
+            pltpu.VMEM(mixed.shape, f32),
+            pltpu.VMEM(log_sums.shape, f32),
+            dma((CHUNKS + 1,)),
+            dma((CHUNKS + 1,)),
+        ],
+        compiler_params=pltpu.CompilerParams(vmem_limit_bytes=VMEM_LIMIT),
+        name="deliver",
+    )(mixed, log_sums)
 
 
 def solution(mesh):

time: 50.5 us -> 50 us (0.990)
  local copies, waits for them, and re-layouts: 2.9 us -> 0 us
  Pallas kernels: 46.8 us -> 49 us
    unnamed x4 -> x0, local copies, waits for them, and re-layouts: 2.9 us -> none
    pallas_call x0 -> x1, Pallas kernels: none -> 2 us  [on_device(): pl.pallas_call(deliver, out_shape=(jax.ShapeDtypeStruct(mixed.shape, f32)...]
where the time goes in v6:
time: 50 us; the launch traced here: 49.8 us
  Pallas kernels  49 us (98%)
  between operations  0.81 us (2%)
    pallas_call x1, Pallas kernels, on_device(): pl.pallas_call(functools.partial(layer, sp, tp, comp, heads), out_shape=(...  47 us
    pallas_call x1, Pallas kernels, on_device(): pl.pallas_call(deliver, out_shape=(jax.ShapeDtypeStruct(mixed.shape, f32)...  2 us

profile of v6, /device:TPU:17, one launch (start us, length us, event | category | flops | bytes accessed | tf_op | source)
XLA Modules:
  0.0 49.8 jit_solution(3632518370939951104)
XLA Ops:
  0.6 47.0 %layer.1 = (f32[128,2048]{1,0:T(8,128)}, f32[2,2,512]{2,1,0:T(2,128)}) custom-call(bf16[128,2048]{1,0:T(8,128)(2,1)} %x_in.1, f32[1,2048]{1,0:T(1,128)} %bitcast.3, f32[2,64]{1,0:T(2,128)} %qg_in.1, f32[2,64]{1,0:T(2,128)} %kg_in.1, f32[2]{0:T(128)} %lam_in.1, f32[1,128]{1,0:T(1,128)} %bitcast.5, f32[3,256]{1,0:T(4,128)} %taps_in.1, f32[1,256]{1,0:T(1,128)} %bitcast.4, ...), custom_call_target="tpu_custom_call" | custom-call | tf_op jit(solution)/shard_map/layer/pallas_call | solution.py:999
  47.7 2.0 %deliver.1 = (f32[128,2048]{1,0:T(8,128)}, f32[2,2,512]{2,1,0:T(2,128)}) custom-call(f32[128,2048]{1,0:T(8,128)} %get-tuple-element.4.mixed_in, f32[2,2,512]{2,1,0:T(2,128)} %get-tuple-element.5.log_in), custom_call_target="tpu_custom_call" | custom-call | tf_op jit(solution)/shard_map/deliver/pallas_call | solution.py:1057
